TPU v7x, 256 devices: a 4x2x16 block of a 4x16x16 slice. The times are simulated.
256 devices in a mesh: grp: 2 (over y), sp: 16 (over z), tp: 4 (over x), dp: 2 (over core).
Axes of the slice: x: 4, y: 2, z: 16, core: 2. Of those that a mesh axis runs over, the one named last changes fastest.
The devices are a block of a 4x16x16 slice.
Arguments:
- latent: bfloat16 [4, 6144, 2048], P(('grp', 'dp'), ('sp', 'tp')), parts along dimension 0, may hold values from -6 to 6
- cond: bfloat16 [4, 2048], P(('grp', 'dp')), parts along dimension 0, may hold values from -6 to 6
- context: bfloat16 [4, 256, 2048], P(('grp', 'dp'), 'sp'), parts along dimension 0, may hold values from -6 to 6
- cond_ctx: bfloat16 [2048], replicated, may hold values from -8 to 8
- w_shift: bfloat16 [2048, 2048], P('sp', 'tp'), may hold values from -0.125 to 0.125
- w_scale: bfloat16 [2048, 2048], P('sp', 'tp'), may hold values from -0.125 to 0.125
- w_gate: bfloat16 [2048, 2048], P('sp', 'tp'), may hold values from -0.125 to 0.125
- norm_gain: float32 [2048], replicated, may hold values from 0.1 to 1.9
- w_query: bfloat16 [2048, 1024], P(None, 'tp'), may hold values from -0.125 to 0.125
- w_key: bfloat16 [2048, 512], P(None, 'tp'), may hold values from -0.125 to 0.125
- w_value: bfloat16 [2048, 512], P(None, 'tp'), may hold values from -0.125 to 0.125
- query_gain: float32 [128], replicated, may hold values from 0.6 to 16
- key_gain: float32 [128], replicated, may hold values from 0.6 to 16
- ctx_lift: float32 [8], P('tp'), may hold values from -2 to 0.5
- out_gain: float32 [1024], replicated, may hold values from 0.1 to 1.9
- w_out: bfloat16 [1024, 2048], replicated, may hold values from -0.1875 to 0.1875
Outputs:
- result: bfloat16 [4, 6144, 2048], P(('grp', 'dp'), ('sp', 'tp')), parts along dimension 0
There are 2 independent parts, one for each index of `grp`. A program takes and returns all parts, laid end to end along the dimension named above; an argument that names none is the same for every part. Nothing has to cross between parts.
All inputs are finite; a program needn't handle non-finite values.
Results may differ from a plain program's by a relative error of at most 0.023.
The roundings to bfloat16 on the way count: a program that leaves them out, or rounds other values in their place, can miss the bound.
Values may be sent and summed in bfloat16 or wider, within the bound.
No kernel may reach another device: no remote copies, remote signals or barrier semaphores. Data moves between devices by JAX's collectives and lax.ppermute only.
A program may use at most 64 MiB of HBM per device.

v0:
```python
import functools
import math

import jax
import jax.numpy as jnp
from jax import lax
from jax.experimental import pallas as pl
from jax.experimental.pallas import tpu as pltpu
from jax.sharding import PartitionSpec as P


HEADS = 8
HEAD_DIM = 128
GRID_WIDTH = 64
EPSILON = 1e-06
FACTOR = HEAD_DIM ** (-0.5)
LOG2E = math.log2(math.e)
F32 = jnp.float32
BF16 = jnp.bfloat16
MIB = 1 << 20


def local_call(body, outs, *, flops, limit=12, scratch=(), aliases=None):
    single = not isinstance(outs, (tuple, list))
    shapes = [outs] if single else list(outs)
    space = pl.BlockSpec(memory_space=pltpu.VMEM)

    def run(*args):
        moved = sum(a.size * a.dtype.itemsize for a in args)
        moved += sum(math.prod(o.shape) * o.dtype.itemsize for o in shapes)
        return pl.pallas_call(
            body,
            out_shape=outs if single else tuple(shapes),
            in_specs=[space] * len(args),
            out_specs=space if single else tuple([space] * len(shapes)),
            scratch_shapes=list(scratch),
            input_output_aliases=aliases or {},
            compiler_params=pltpu.CompilerParams(vmem_limit_bytes=limit * MIB),
            cost_estimate=pl.CostEstimate(
                flops=flops, bytes_accessed=moved, transcendentals=0
            ),
        )(*args)

    return run


FAR = pl.BlockSpec(memory_space=pltpu.MemorySpace.HBM)


def far(x):
    return pltpu.with_memory_space_constraint(x, pltpu.MemorySpace.HBM)


def shape(dims, dtype):
    return jax.ShapeDtypeStruct(dims, dtype)


def modulation_kernel(cond, cond_ctx, wa, wb, wc, out_ref, weights, sem):
    copies = [
        pltpu.make_async_copy(w, weights.at[i], sem.at[i]) for i, w in enumerate((wa, wb, wc))
    ]
    for copy in copies:
        copy.start()
    depth = weights.shape[1]
    at = pl.ds(pl.multiple_of(lax.axis_index("sp") * depth, depth), depth)
    rows = jnp.concatenate([cond[:, at].astype(F32), cond_ctx[:, at].astype(F32)], 0)
    acted = (rows * jax.nn.sigmoid(rows)).astype(BF16)
    for copy in copies:
        copy.wait()
    shift, scale, gate = (
        jnp.dot(acted, weights[i], preferred_element_type=F32) for i in range(3)
    )
    mod = jnp.concatenate([shift[0:1], scale[0:1], shift[1:2], scale[1:2]], 0)
    part = gate.shape[1] // 4
    gate = jnp.concatenate([gate[0:1, i * part : (i + 1) * part] for i in range(4)], 0)
    mod = jnp.concatenate([mod, gate], 1)
    for i in range(out_ref.shape[0]):
        out_ref[i] = mod


def sum_kernel(parts, out_ref):
    total = jnp.sum(parts[...], 0)
    for i in range(out_ref.shape[0]):
        out_ref[i] = total


def kv_kernel(
    x0, x1, x2, x3, ctx, mod, gain, wkv, key_gain, cosine, sine, chunk_ref, normed_ref
):
    wide = gain.shape[1] // mod.shape[0]

    def row_of(index):
        return jnp.concatenate([mod[b, index : index + 1, :wide] for b in range(mod.shape[0])], 1)

    gains = gain[...]
    amp, shift = gains * (1.0 + row_of(1)), row_of(0)

    def norm(rows, amp, shift):
        rows = rows.astype(F32)
        mean = jnp.mean(rows * rows, -1, keepdims=True)
        return (rows * lax.rsqrt(mean + EPSILON) * amp + shift).astype(BF16)

    ctx_rows = ctx.shape[0]
    normed_ref[0:ctx_rows, :] = norm(ctx[...], gains * (1.0 + row_of(3)), row_of(2))
    own = x0.shape[0]
    for block, x in enumerate((x0, x1, x2, x3)):
        for t in range(own // 16):
            at = ctx_rows + block * own + t * 16
            normed_ref[at : at + 16, :] = norm(x[t * 16 : t * 16 + 16, :], amp, shift)
    kv = jnp.dot(normed_ref[...], wkv[...], preferred_element_type=F32)
    chunk_ref[1] = kv[:, HEAD_DIM:].astype(BF16)
    k = head_norm(kv[:, :HEAD_DIM], key_gain[...])
    chunk_ref[0, 0:ctx_rows, :] = k[0:ctx_rows].astype(BF16)
    chunk_ref[0, ctx_rows:, :] = rotate(k[ctx_rows:], cosine[...], sine[...]).astype(BF16)


def head_norm(vectors, gain):
    floats = vectors.astype(BF16).astype(F32)
    return floats * lax.rsqrt(jnp.mean(floats * floats, -1, keepdims=True) + EPSILON) * gain


def rotate(vectors, cosine, signed_sine):
    lanes = vectors.shape[-1]
    quarter = lanes // 4
    lane = lax.broadcasted_iota(jnp.int32, vectors.shape, 1)
    up = pltpu.roll(vectors, lanes - quarter, 1)
    down = pltpu.roll(vectors, quarter, 1)
    partner = jnp.where(lane % (2 * quarter) < quarter, up, down)
    return vectors * cosine + partner * signed_sine


def query_kernel(normed, wq, query_gain, cosine, sine, out_ref):
    rows = cosine.shape[0]
    skip = normed.shape[0] - rows
    q = jnp.dot(normed[skip:, :], wq[...], preferred_element_type=F32)
    for h in range(q.shape[1] // HEAD_DIM):
        one = head_norm(q[:, h * HEAD_DIM : (h + 1) * HEAD_DIM], query_gain[...])
        one = rotate(one, cosine[...], sine[...])
        out_ref[:, h * rows : (h + 1) * rows] = one.T.astype(BF16)


def attend_kernel(ctx_rows, first, pairs, *refs):
    refs = list(refs)
    qt, lift = refs[0], refs[1]
    if pairs:
        chunks = [(refs[2], refs[3])]
        rest = refs[4:]
    else:
        count = len(refs) - 2 - (2 if first else 4)
        chunks = [(r.at[0], r.at[1]) for r in refs[2 : 2 + count]]
        rest = refs[2 + count :]
    if first:
        acc_out, stat_out = rest
    else:
        acc_in, stat_in, acc_out, stat_out = rest
    total = qt.shape[1]
    width = 256
    for begin in range(0, total, width):
        part = slice(begin, begin + width)
        q = qt[:, part]
        bias = lift[:, part]
        if first:
            top = low = acc = None
        else:
            top, low, acc = stat_in[0:1, part], stat_in[1:2, part], acc_in[:, part]
        for k_ref, v_ref in chunks:
            s = jnp.dot(k_ref[...], q, preferred_element_type=F32)
            s = jnp.concatenate([s[:ctx_rows] + bias, s[ctx_rows:]], 0)
            new = jnp.max(s, 0, keepdims=True)
            if top is not None:
                new = jnp.maximum(top, new)
            p = jnp.exp2((s - new) * (FACTOR * LOG2E))
            size = jnp.sum(p, 0, keepdims=True)
            mixed = lax.dot_general(
                v_ref[...], p.astype(BF16), (((0,), (0,)), ((), ())), preferred_element_type=F32
            )
            if top is None:
                low, acc = size, mixed
            else:
                keep = jnp.exp2((top - new) * (FACTOR * LOG2E))
                low, acc = low * keep + size, acc * keep + mixed
            top = new
        acc_out[:, part] = acc
        stat_out[0:1, part] = top
        stat_out[1:2, part] = low


def finish_kernel(acc, stat, *targets):
    own = targets[0].shape[0]
    rows = len(targets) * own
    for h in range(acc.shape[1] // rows):
        part = slice(h * rows, (h + 1) * rows)
        att = (acc[:, part] / stat[1:2, part]).T.astype(BF16)
        for b, target in enumerate(targets):
            target[:, h * HEAD_DIM : (h + 1) * HEAD_DIM] = att[b * own : (b + 1) * own]


def out_kernel(order, a0, a1, a2, a3, gain, w_out, latent, mod, out_ref, weights, sem):
    blocks = mod.shape[0]
    wide = out_ref.shape[1] // blocks
    copies = [
        pltpu.make_async_copy(w_out.at[:, pl.ds(b * wide, wide)], weights.at[b], sem.at[b])
        for b in range(blocks)
    ]
    for copy in copies:
        copy.start()
    cols = a0.shape[1]
    atts = [a[...].astype(F32) for a in (a0, a1, a2, a3)]
    total = sum(jnp.sum(a * a, -1, keepdims=True) for a in atts)
    scale = lax.rsqrt(total / (cols * len(atts)) + EPSILON)
    normed = [
        (a * scale * gain[pl.ds(order[i], 1), :]).astype(BF16) for i, a in enumerate(atts)
    ]
    for b in range(blocks):
        copies[b].wait()
        part = slice(b * wide, (b + 1) * wide)
        mix = 0.0
        for i, a in enumerate(normed):
            at = pl.multiple_of(order[i] * cols, cols)
            mix += jnp.dot(a, weights[b, pl.ds(at, cols), :], preferred_element_type=F32)
        gate = jnp.concatenate([mod[b, r : r + 1, wide:] for r in range(mod.shape[1])], 1)
        out = latent[:, part].astype(F32) + gate * mix
        out_ref[:, part] = out.astype(BF16)


def angles(positions):
    freqs = HEAD_DIM // 4
    rows = (positions // GRID_WIDTH).astype(F32)
    cols = (positions % GRID_WIDTH).astype(F32)
    inverse = 10000.0 ** (-jnp.arange(freqs, dtype=F32) / freqs)
    by_row, by_col = rows[:, None] * inverse, cols[:, None] * inverse
    cosine = [jnp.cos(by_row)] * 2 + [jnp.cos(by_col)] * 2
    sine = [-jnp.sin(by_row), jnp.sin(by_row), -jnp.sin(by_col), jnp.sin(by_col)]
    return jnp.concatenate(cosine, 1), jnp.concatenate(sine, 1)


def shifted(x, axis, by):
    count = lax.axis_size(axis)
    return lax.ppermute(x, axis, [(i, (i + by) % count) for i in range(count)])


def on_device(
    latent,
    cond,
    context,
    cond_ctx,
    w_shift,
    w_scale,
    w_gate,
    norm_gain,
    w_query,
    w_key,
    w_value,
    query_gain,
    key_gain,
    ctx_lift,
    out_gain,
    w_out,
):
    sp, tp = lax.axis_index("sp"), lax.axis_index("tp")
    n_sp, n_tp = lax.axis_size("sp"), lax.axis_size("tp")
    own_rows, width = latent.shape[1:]
    latent, context = latent[0], context[0]
    ctx_rows = context.shape[0]
    rows = own_rows * n_tp
    in_rows, out_cols = w_shift.shape

    space = pl.BlockSpec(memory_space=pltpu.VMEM)
    packed = (4, out_cols + out_cols // 4)
    parts = pl.pallas_call(
        modulation_kernel,
        out_shape=shape((n_sp, *packed), F32),
        in_specs=[space, space, FAR, FAR, FAR],
        out_specs=space,
        scratch_shapes=[
            pltpu.VMEM((3, in_rows, out_cols), BF16),
            pltpu.SemaphoreType.DMA((3,)),
        ],
        compiler_params=pltpu.CompilerParams(vmem_limit_bytes=4 * MIB),
        cost_estimate=pl.CostEstimate(flops=10**6, bytes_accessed=MIB, transcendentals=0),
        name="modulation",
    )(cond, cond_ctx[None], far(w_shift), far(w_scale), far(w_gate))
    parts = lax.all_to_all(parts, "sp", 0, 0)
    mod = local_call(sum_kernel, shape((n_tp, *packed), F32), flops=10**6, limit=4)(parts)
    mod = lax.all_to_all(mod, "tp", 0, 0)

    latents = [latent]
    for by in (1, -1, 2):
        latents.append(shifted(latent, "tp", by))
    owners = jnp.stack([tp, (tp - 1) % n_tp, (tp + 1) % n_tp, (tp + 2) % n_tp])
    positions = sp * rows + (owners[:, None] * own_rows + jnp.arange(own_rows)[None]).reshape(-1)
    cosine, sine = angles(positions.astype(jnp.int32))
    wkv = jnp.concatenate([w_key, w_value], 1)
    length = ctx_rows + rows
    chunk, normed = local_call(
        kv_kernel,
        (shape((2, length, HEAD_DIM), BF16), shape((length, width), BF16)),
        flops=2 * length * width * 256,
        limit=16,
    )(*latents, context, mod, norm_gain[None], wkv, key_gain[None], cosine, sine)
    q_cols = w_query.shape[1]
    group = q_cols // HEAD_DIM
    qt = local_call(
        query_kernel, shape((HEAD_DIM, group * rows), BF16), flops=2 * rows * width * q_cols, limit=16
    )(normed, w_query, query_gain[None], cosine, sine)
    lift = (ctx_lift + math.log(rows / ctx_rows)) / FACTOR
    lift = jnp.repeat(lift, rows)[None]

    lanes = group * rows
    state_shapes = (shape((HEAD_DIM, lanes), F32), shape((2, lanes), F32))
    state = local_call(
        functools.partial(attend_kernel, ctx_rows, True, False),
        state_shapes,
        flops=4 * length * lanes * HEAD_DIM,
    )(qt, lift, chunk)

    def attend(state, *chunks, pairs=False):
        count = 1 if pairs else len(chunks)
        given = (qt, lift, *chunks, *state)
        return local_call(
            functools.partial(attend_kernel, ctx_rows, False, pairs),
            state_shapes,
            flops=4 * count * length * lanes * HEAD_DIM,
            aliases={len(given) - 2: 0, len(given) - 1: 1},
        )(*given)

    right, left = shifted(chunk, "sp", 1), shifted(chunk, "sp", -1)
    for _ in range(n_sp // 2 - 2):
        right, left, state = lax.optimization_barrier((right, left, state))
        arrived = right, left
        right, left = shifted(right, "sp", 1), shifted(left, "sp", -1)
        state = attend(state, *arrived)
    right, left, state = lax.optimization_barrier((right, left, state))
    last_k, last_v = shifted(right[0], "sp", 1), shifted(left[1], "sp", -1)
    state = attend(state, right, left)
    state = attend(state, last_k, last_v, pairs=True)

    own, to_left, to_right, to_far = local_call(
        finish_kernel, [shape((own_rows, q_cols), BF16)] * n_tp, flops=10**6
    )(*state)
    atts = [own, shifted(to_left, "tp", -1), shifted(to_right, "tp", 1), shifted(to_far, "tp", 2)]
    order = jnp.stack([tp, (tp + 1) % n_tp, (tp - 1) % n_tp, (tp + 2) % n_tp]).astype(jnp.int32)
    result = pl.pallas_call(
        out_kernel,
        out_shape=shape((own_rows, width), BF16),
        in_specs=[pl.BlockSpec(memory_space=pltpu.SMEM)] + [space] * 5 + [FAR, space, space],
        out_specs=space,
        scratch_shapes=[
            pltpu.VMEM((n_tp, w_out.shape[0], out_cols), BF16),
            pltpu.SemaphoreType.DMA((n_tp,)),
        ],
        compiler_params=pltpu.CompilerParams(vmem_limit_bytes=12 * MIB),
        cost_estimate=pl.CostEstimate(
            flops=2 * own_rows * width * HEADS * HEAD_DIM, bytes_accessed=5 * MIB, transcendentals=0
        ),
        name="output",
    )(order, *atts, out_gain.reshape(n_tp, q_cols), far(w_out), latent, mod)
    return result[None]


def solution(mesh):
    in_specs = (
        P(("grp", "dp"), ("sp", "tp"), None),
        P(("grp", "dp"), None),
        P(("grp", "dp"), "sp", None),
        P(),
        P("sp", "tp"),
        P("sp", "tp"),
        P("sp", "tp"),
        P(),
        P(None, "tp"),
        P(None, "tp"),
        P(None, "tp"),
        P(),
        P(),
        P("tp"),
        P(),
        P(),
    )
    out_specs = P(("grp", "dp"), ("sp", "tp"), None)


    return jax.shard_map(
        on_device, mesh=mesh, in_specs=in_specs, out_specs=out_specs, check_vma=False
    )
```

profile of v0, /device:TPU:40, one launch (start us, length us, event | category | flops | bytes accessed | tf_op | source)
XLA Modules:
  0.0 133.0 jit_solution(9180598815301590819)
XLA Ops:
  0.0 1.6 %collective-permute-start = (bf16[96,2048]{1,0:T(8,128)(2,1)}, bf16[96,2048]{1,0:T(8,128)(2,1)S(1)}, u32[]{:S(2)}, u32[]{:S(2)}) collective-permute-start(bf16[96,2048]{1,0:T(8,128)(2,1)} %bitcast.18), channel_id=1, source_target_pairs={{0,2},{2,4},{4,6},{6,0},{1,3},{3,5},{5,7},{7,1},{8,10},{10,12},{12... | collective-permute-start | bytes 1179656 | tf_op jit(solution)/shard_map/ppermute | solution.py:239
  1.6 1.6 %collective-permute-start.1 = (bf16[96,2048]{1,0:T(8,128)(2,1)}, bf16[96,2048]{1,0:T(8,128)(2,1)}, u32[]{:S(2)}, u32[]{:S(2)}) collective-permute-start(bf16[96,2048]{1,0:T(8,128)(2,1)} %bitcast.19), channel_id=1, source_target_pairs={{0,6},{2,0},{4,2},{6,4},{1,7},{3,1},{5,3},{7,5},{8,14},{10,8},{12,... | collective-permute-start | bytes 1179656 | tf_op jit(solution)/shard_map/ppermute | solution.py:239
  3.2 2.1 %collective-permute-start.2 = (bf16[96,2048]{1,0:T(8,128)(2,1)}, bf16[96,2048]{1,0:T(8,128)(2,1)}, u32[]{:S(2)}, u32[]{:S(2)}) collective-permute-start(bf16[96,2048]{1,0:T(8,128)(2,1)} %bitcast.20), channel_id=1, source_target_pairs={{0,4},{2,6},{4,0},{6,2},{1,5},{3,7},{5,1},{7,3},{8,12},{10,14},{12... | collective-permute-start | bytes 1179656 | tf_op jit(solution)/shard_map/ppermute | solution.py:239
  6.7 1.9 %modulation.1 = f32[16,4,640]{2,1,0:T(4,128)} custom-call(bf16[1,2048]{1,0:T(2,128)(2,1)S(1)} %copy-done.3, bf16[1,2048]{1,0:T(2,128)(2,1)S(1)} %broadcast_in_dim.24.cond_ctx, bf16[128,512]{1,0:T(8,128)(2,1)} %wa.1, bf16[128,512]{1,0:T(8,128)(2,1)} %wb.1, bf16[128,512]{1,0:T(8,128)(2,1)} %wc.1), custom_call_target="tpu_custom_call" | custom-call | flops 1000000 | bytes 1048576 | tf_op jit(solution)/shard_map/modulation/pallas_call | solution.py:270
  8.6 24.0 %all-to-all-start = ((f32[16,4,640]{2,1,0:T(4,128)}), f32[16,4,640]{2,1,0:T(4,128)S(1)}, u32[]{:S(2)}, u32[]{:S(2)}) async-start(f32[16,4,640]{2,1,0:T(4,128)} %modulation.1), calls=%async_computation | async-start | bytes 327680 | tf_op jit(solution)/shard_map/all_to_all | solution.py:283
  33.6 1.4 %pad_maximum_fusion.wkv = bf16[2048,256]{1,0:T(8,128)(2,1)S(1)} fusion(bf16[2048,128]{1,0:T(8,128)(2,1)} %param.26, bf16[2048,128]{1,0:T(8,128)(2,1)} %param.25), kind=kLoop, calls=%fused_computation | loop fusion | flops 2097152 | bytes 2097152 | tf_op jit(solution)/shard_map/concatenate | solution.py:293
  35.0 2.5 %fusion = (f32[384,32]{1,0:T(8,128)}, f32[384,32]{1,0:T(8,128)}, f32[384,32]{1,0:T(8,128)}, f32[384,32]{1,0:T(8,128)}, f32[384,32]{1,0:T(8,128)}, /*index=5*/f32[384,32]{1,0:T(8,128)}) fusion(f32[32]{0:T(128)S(1)} %multiply_power_fusion, f32[384]{0:T(512)S(1)} %get-tuple-element.115, f32[384]{0:T(512)S(1)} %get-tuple-element.116), kind=kLoop, calls=%fused_computation.9 | loop fusion | flops 49152 | bytes 298112 | tf_op jit(solution)/shard_map/neg | solution.py:233
  37.4 10.0 %all-to-all-done.parts = f32[16,4,640]{2,1,0:T(4,128)S(1)} async-done(((f32[16,4,640]{2,1,0:T(4,128)}), f32[16,4,640]{2,1,0:T(4,128)S(1)}, u32[]{:S(2)}, u32[]{:S(2)}) %all-to-all-start) | async-done | bytes 163872 | tf_op jit(solution)/shard_map/all_to_all | solution.py:283
  48.1 3.4 %all-to-all-start.1 = ((f32[4,4,640]{2,1,0:T(4,128)}), f32[4,4,640]{2,1,0:T(4,128)S(1)}, u32[]{:S(2)}, u32[]{:S(2)}) async-start(f32[4,4,640]{2,1,0:T(4,128)} %shard_map.154), calls=%async_computation.1 | async-start | bytes 81920 | tf_op jit(solution)/shard_map/all_to_all | solution.py:285
  51.5 1.9 %pad_maximum_fusion.1 = (f32[384,128]{1,0:T(8,128)S(1)}, f32[384,128]{1,0:T(8,128)S(1)}) fusion(f32[384,32]{1,0:T(8,128)} %get-tuple-element.118, f32[384,32]{1,0:T(8,128)} %get-tuple-element.111, f32[384,32]{1,0:T(8,128)} %get-tuple-element.117, f32[384,32]{1,0:T(8,128)} %get-tuple-element.119, f32[384,32]{1,0:T(8,128)} %get-tuple-element.110, ...), kind=kLoop, calls=%fused_computation.5 | loop fusion | flops 294912 | bytes 688128 | tf_op jit(solution)/shard_map/concatenate | solution.py:234
  53.4 3.4 %all-to-all-done.1.mod = f32[4,4,640]{2,1,0:T(4,128)S(1)} async-done(((f32[4,4,640]{2,1,0:T(4,128)}), f32[4,4,640]{2,1,0:T(4,128)S(1)}, u32[]{:S(2)}, u32[]{:S(2)}) %all-to-all-start.1) | async-done | bytes 40992 | tf_op jit(solution)/shard_map/all_to_all | solution.py:285
  56.9 2.3 %shard_map.155 = (bf16[2,400,128]{2,1,0:T(8,128)(2,1)S(1)}, bf16[400,2048]{1,0:T(8,128)(2,1)S(1)}) custom-call(bf16[96,2048]{1,0:T(8,128)(2,1)S(1)} %bitcast.21, bf16[96,2048]{1,0:T(8,128)(2,1)S(1)} %collective-permute-done.x1, bf16[96,2048]{1,0:T(8,128)(2,1)} %collective-permute-done.1.x2, bf16[96,2048]{1,0:T(8,128)(2,1)} %collective-permute-done.2.x3, ...), custom_call_target="tpu_custom_call" | custom-call | flops 419430400 | bytes 4973056 | tf_op jit(solution)/shard_map/pallas_call | solution.py:31
  59.2 1.5 %collective-permute-start.3 = (bf16[2,400,128]{2,1,0:T(8,128)(2,1)S(1)}, bf16[2,400,128]{2,1,0:T(8,128)(2,1)S(1)}, u32[]{:S(2)}, u32[]{:S(2)}) collective-permute-start(bf16[2,400,128]{2,1,0:T(8,128)(2,1)S(1)} %get-tuple-element.58.refs_2_), channel_id=1, source_target_pairs={{0,8},{8,16},{16,24},{24,32},{32,40},{40,48},{48,56},{56,64},{64,7... | collective-permute-start | bytes 614408 | tf_op jit(solution)/shard_map/ppermute | solution.py:239
  60.6 1.9 %collective-permute-start.4 = (bf16[2,400,128]{2,1,0:T(8,128)(2,1)S(1)}, bf16[2,400,128]{2,1,0:T(8,128)(2,1)S(1)}, u32[]{:S(2)}, u32[]{:S(2)}) collective-permute-start(bf16[2,400,128]{2,1,0:T(8,128)(2,1)S(1)} %get-tuple-element.58.refs_2_), channel_id=1, source_target_pairs={{0,120},{8,0},{16,8},{24,16},{32,24},{40,32},{48,40},{56,48},{64,5... | collective-permute-start | bytes 614408 | tf_op jit(solution)/shard_map/ppermute | solution.py:239
  62.6 1.1 shard_map.156.refs_0_
  63.7 1.2 shard_map.157
  65.0 3.4 %collective-permute-done.3.refs_2_ = bf16[2,400,128]{2,1,0:T(8,128)(2,1)S(1)} collective-permute-done((bf16[2,400,128]{2,1,0:T(8,128)(2,1)S(1)}, bf16[2,400,128]{2,1,0:T(8,128)(2,1)S(1)}, u32[]{:S(2)}, u32[]{:S(2)}) %collective-permute-start.3) | collective-permute-done | bytes 204832 | tf_op jit(solution)/shard_map/ppermute | solution.py:239
  68.6 3.2 %collective-permute-start.6 = (bf16[2,400,128]{2,1,0:T(8,128)(2,1)S(1)}, bf16[2,400,128]{2,1,0:T(8,128)(2,1)S(1)}, u32[]{:S(2)}, u32[]{:S(2)}) collective-permute-start(bf16[2,400,128]{2,1,0:T(8,128)(2,1)S(1)} %collective-permute-done.4.refs_3_), channel_id=1, source_target_pairs={{0,120},{8,0},{16,8},{24,16},{32,24},{40,32},{48,40},{56,48},{64,5... | collective-permute-start | bytes 614408 | tf_op jit(solution)/shard_map/ppermute | solution.py:239
  71.8 2.3 %shard_map.158 = (f32[128,768]{1,0:T(8,128)S(1)}, f32[2,768]{1,0:T(2,128)S(1)}) custom-call(bf16[128,768]{1,0:T(8,128)(2,1)S(1)} %shard_map.156.refs_0_, f32[1,768]{1,0:T(1,128)S(1)} %bitcast.25, bf16[2,400,128]{2,1,0:T(8,128)(2,1)S(1)} %collective-permute-done.3.refs_2_, ...), custom_call_target="tpu_custom_call", output_to_operand_aliasing={{0}: (4, {}), {1}: (5, {})} | custom-call | flops 314572800 | bytes 1408000 | tf_op jit(solution)/shard_map/pallas_call | solution.py:31
  74.1 2.8 %collective-permute-done.5.refs_2_ = bf16[2,400,128]{2,1,0:T(8,128)(2,1)S(1)} collective-permute-done((bf16[2,400,128]{2,1,0:T(8,128)(2,1)S(1)}, bf16[2,400,128]{2,1,0:T(8,128)(2,1)S(1)}, u32[]{:S(2)}, u32[]{:S(2)}) %collective-permute-start.5) | collective-permute-done | bytes 204832 | tf_op jit(solution)/shard_map/ppermute | solution.py:239
  76.9 3.2 %collective-permute-start.8 = (bf16[2,400,128]{2,1,0:T(8,128)(2,1)S(1)}, bf16[2,400,128]{2,1,0:T(8,128)(2,1)S(1)}, u32[]{:S(2)}, u32[]{:S(2)}) collective-permute-start(bf16[2,400,128]{2,1,0:T(8,128)(2,1)S(1)} %collective-permute-done.6.refs_3_), channel_id=1, source_target_pairs={{0,120},{8,0},{16,8},{24,16},{32,24},{40,32},{48,40},{56,48},{64,5... | collective-permute-start | bytes 614408 | tf_op jit(solution)/shard_map/ppermute | solution.py:239
  80.1 2.3 %shard_map.159 = (f32[128,768]{1,0:T(8,128)S(1)}, f32[2,768]{1,0:T(2,128)S(1)}) custom-call(bf16[128,768]{1,0:T(8,128)(2,1)S(1)} %shard_map.156.refs_0_, f32[1,768]{1,0:T(1,128)S(1)} %bitcast.26, bf16[2,400,128]{2,1,0:T(8,128)(2,1)S(1)} %collective-permute-done.5.refs_2_, ...), custom_call_target="tpu_custom_call", output_to_operand_aliasing={{0}: (4, {}), {1}: (5, {})} | custom-call | flops 314572800 | bytes 1408000 | tf_op jit(solution)/shard_map/pallas_call | solution.py:31
  82.4 1.9 %collective-permute-done.7.refs_2_ = bf16[2,400,128]{2,1,0:T(8,128)(2,1)S(1)} collective-permute-done((bf16[2,400,128]{2,1,0:T(8,128)(2,1)S(1)}, bf16[2,400,128]{2,1,0:T(8,128)(2,1)S(1)}, u32[]{:S(2)}, u32[]{:S(2)}) %collective-permute-start.7) | collective-permute-done | bytes 204832 | tf_op jit(solution)/shard_map/ppermute | solution.py:239
  84.3 1.0 collective-permute-start.9
  85.4 2.2 %collective-permute-start.10 = (bf16[2,400,128]{2,1,0:T(8,128)(2,1)S(1)}, bf16[2,400,128]{2,1,0:T(8,128)(2,1)S(1)}, u32[]{:S(2)}, u32[]{:S(2)}) collective-permute-start(bf16[2,400,128]{2,1,0:T(8,128)(2,1)S(1)} %collective-permute-done.8.refs_3_), channel_id=1, source_target_pairs={{0,120},{8,0},{16,8},{24,16},{32,24},{40,32},{48,40},{56,48},{64,5... | collective-permute-start | bytes 614408 | tf_op jit(solution)/shard_map/ppermute | solution.py:239
  87.6 2.3 %shard_map.160 = (f32[128,768]{1,0:T(8,128)S(1)}, f32[2,768]{1,0:T(2,128)S(1)}) custom-call(bf16[128,768]{1,0:T(8,128)(2,1)S(1)} %shard_map.156.refs_0_, f32[1,768]{1,0:T(1,128)S(1)} %bitcast.27, bf16[2,400,128]{2,1,0:T(8,128)(2,1)S(1)} %collective-permute-done.7.refs_2_, ...), custom_call_target="tpu_custom_call", output_to_operand_aliasing={{0}: (4, {}), {1}: (5, {})} | custom-call | flops 314572800 | bytes 1408000 | tf_op jit(solution)/shard_map/pallas_call | solution.py:31
  89.9 1.4 %collective-permute-done.9.refs_2_ = bf16[2,400,128]{2,1,0:T(8,128)(2,1)S(1)} collective-permute-done((bf16[2,400,128]{2,1,0:T(8,128)(2,1)S(1)}, bf16[2,400,128]{2,1,0:T(8,128)(2,1)S(1)}, u32[]{:S(2)}, u32[]{:S(2)}) %collective-permute-start.9) | collective-permute-done | bytes 204832 | tf_op jit(solution)/shard_map/ppermute | solution.py:239
  91.3 1.3 collective-permute-start.11
  92.6 1.9 %collective-permute-start.12 = (bf16[2,400,128]{2,1,0:T(8,128)(2,1)S(1)}, bf16[2,400,128]{2,1,0:T(8,128)(2,1)S(1)}, u32[]{:S(2)}, u32[]{:S(2)}) collective-permute-start(bf16[2,400,128]{2,1,0:T(8,128)(2,1)S(1)} %collective-permute-done.10.refs_3_), channel_id=1, source_target_pairs={{0,120},{8,0},{16,8},{24,16},{32,24},{40,32},{48,40},{56,48},{64,5... | collective-permute-start | bytes 614408 | tf_op jit(solution)/shard_map/ppermute | solution.py:239
  94.5 2.3 %shard_map.161 = (f32[128,768]{1,0:T(8,128)S(1)}, f32[2,768]{1,0:T(2,128)S(1)}) custom-call(bf16[128,768]{1,0:T(8,128)(2,1)S(1)} %shard_map.156.refs_0_, f32[1,768]{1,0:T(1,128)S(1)} %bitcast.28, bf16[2,400,128]{2,1,0:T(8,128)(2,1)S(1)} %collective-permute-done.9.refs_2_, ...), custom_call_target="tpu_custom_call", output_to_operand_aliasing={{0}: (4, {}), {1}: (5, {})} | custom-call | flops 314572800 | bytes 1408000 | tf_op jit(solution)/shard_map/pallas_call | solution.py:31
  96.9 1.4 %collective-permute-done.11.refs_2_ = bf16[2,400,128]{2,1,0:T(8,128)(2,1)S(1)} collective-permute-done((bf16[2,400,128]{2,1,0:T(8,128)(2,1)S(1)}, bf16[2,400,128]{2,1,0:T(8,128)(2,1)S(1)}, u32[]{:S(2)}, u32[]{:S(2)}) %collective-permute-start.11) | collective-permute-done | bytes 204832 | tf_op jit(solution)/shard_map/ppermute | solution.py:239
  98.4 1.6 %collective-permute-start.13 = (bf16[2,400,128]{2,1,0:T(8,128)(2,1)S(1)}, bf16[2,400,128]{2,1,0:T(8,128)(2,1)S(1)}, u32[]{:S(2)}, u32[]{:S(2)}) collective-permute-start(bf16[2,400,128]{2,1,0:T(8,128)(2,1)S(1)} %collective-permute-done.11.refs_2_), channel_id=1, source_target_pairs={{0,8},{8,16},{16,24},{24,32},{32,40},{40,48},{48,56},{56,64},{64,7... | collective-permute-start | bytes 614408 | tf_op jit(solution)/shard_map/ppermute | solution.py:239
  99.9 1.7 %collective-permute-start.14 = (bf16[2,400,128]{2,1,0:T(8,128)(2,1)S(1)}, bf16[2,400,128]{2,1,0:T(8,128)(2,1)S(1)}, u32[]{:S(2)}, u32[]{:S(2)}) collective-permute-start(bf16[2,400,128]{2,1,0:T(8,128)(2,1)S(1)} %collective-permute-done.12.refs_3_), channel_id=1, source_target_pairs={{0,120},{8,0},{16,8},{24,16},{32,24},{40,32},{48,40},{56,48},{64,5... | collective-permute-start | bytes 614408 | tf_op jit(solution)/shard_map/ppermute | solution.py:239
  101.6 2.3 %shard_map.162 = (f32[128,768]{1,0:T(8,128)S(1)}, f32[2,768]{1,0:T(2,128)S(1)}) custom-call(bf16[128,768]{1,0:T(8,128)(2,1)S(1)} %shard_map.156.refs_0_, f32[1,768]{1,0:T(1,128)S(1)} %bitcast.29, bf16[2,400,128]{2,1,0:T(8,128)(2,1)S(1)} %collective-permute-done.11.refs_2_, ...), custom_call_target="tpu_custom_call", output_to_operand_aliasing={{0}: (4, {}), {1}: (5, {})} | custom-call | flops 314572800 | bytes 1408000 | tf_op jit(solution)/shard_map/pallas_call | solution.py:31
  103.9 1.4 %collective-permute-done.13.refs_2_ = bf16[2,400,128]{2,1,0:T(8,128)(2,1)S(1)} collective-permute-done((bf16[2,400,128]{2,1,0:T(8,128)(2,1)S(1)}, bf16[2,400,128]{2,1,0:T(8,128)(2,1)S(1)}, u32[]{:S(2)}, u32[]{:S(2)}) %collective-permute-start.13) | collective-permute-done | bytes 204832 | tf_op jit(solution)/shard_map/ppermute | solution.py:239
  105.7 2.0 %collective-permute-start.15 = (bf16[2,400,128]{2,1,0:T(8,128)(2,1)S(1)}, bf16[2,400,128]{2,1,0:T(8,128)(2,1)S(1)}, u32[]{:S(2)}, u32[]{:S(2)}) collective-permute-start(bf16[2,400,128]{2,1,0:T(8,128)(2,1)S(1)} %collective-permute-done.13.refs_2_), channel_id=1, source_target_pairs={{0,8},{8,16},{16,24},{24,32},{32,40},{40,48},{48,56},{56,64},{64,7... | collective-permute-start | bytes 614408 | tf_op jit(solution)/shard_map/ppermute | solution.py:239
  107.7 1.2 collective-permute-start.16
  108.9 2.3 %shard_map.163 = (f32[128,768]{1,0:T(8,128)S(1)}, f32[2,768]{1,0:T(2,128)S(1)}) custom-call(bf16[128,768]{1,0:T(8,128)(2,1)S(1)} %shard_map.156.refs_0_, f32[1,768]{1,0:T(1,128)S(1)} %bitcast.30, bf16[2,400,128]{2,1,0:T(8,128)(2,1)S(1)} %collective-permute-done.13.refs_2_, ...), custom_call_target="tpu_custom_call", output_to_operand_aliasing={{0}: (4, {}), {1}: (5, {})} | custom-call | flops 314572800 | bytes 1408000 | tf_op jit(solution)/shard_map/pallas_call | solution.py:31
  111.2 1.4 %collective-permute-done.15.refs_2_ = bf16[2,400,128]{2,1,0:T(8,128)(2,1)S(1)} collective-permute-done((bf16[2,400,128]{2,1,0:T(8,128)(2,1)S(1)}, bf16[2,400,128]{2,1,0:T(8,128)(2,1)S(1)}, u32[]{:S(2)}, u32[]{:S(2)}) %collective-permute-start.15) | collective-permute-done | bytes 204832 | tf_op jit(solution)/shard_map/ppermute | solution.py:239
  113.5 1.6 %collective-permute-start.17 = (bf16[400,128]{1,0:T(8,128)(2,1)S(1)}, bf16[400,128]{1,0:T(8,128)(2,1)S(1)}, u32[]{:S(2)}, u32[]{:S(2)}) collective-permute-start(bf16[400,128]{1,0:T(8,128)(2,1)S(1)} %slice_bitcast_fusion.1), channel_id=1, source_target_pairs={{0,8},{8,16},{16,24},{24,32},{32,40},{40,48},{48,56},{56,64},{64,7... | collective-permute-start | bytes 307208 | tf_op jit(solution)/shard_map/ppermute | solution.py:239
  115.1 1.9 %collective-permute-start.18 = (bf16[400,128]{1,0:T(8,128)(2,1)S(1)}, bf16[400,128]{1,0:T(8,128)(2,1)S(1)}, u32[]{:S(2)}, u32[]{:S(2)}) collective-permute-start(bf16[400,128]{1,0:T(8,128)(2,1)S(1)} %slice_bitcast_fusion), channel_id=1, source_target_pairs={{0,120},{8,0},{16,8},{24,16},{32,24},{40,32},{48,40},{56,48},{64,5... | collective-permute-start | bytes 307208 | tf_op jit(solution)/shard_map/ppermute | solution.py:239
  116.9 2.3 %shard_map.164 = (f32[128,768]{1,0:T(8,128)S(1)}, f32[2,768]{1,0:T(2,128)S(1)}) custom-call(bf16[128,768]{1,0:T(8,128)(2,1)S(1)} %shard_map.156.refs_0_, f32[1,768]{1,0:T(1,128)S(1)} %bitcast.31, bf16[2,400,128]{2,1,0:T(8,128)(2,1)S(1)} %collective-permute-done.15.refs_2_, ...), custom_call_target="tpu_custom_call", output_to_operand_aliasing={{0}: (4, {}), {1}: (5, {})} | custom-call | flops 314572800 | bytes 1408000 | tf_op jit(solution)/shard_map/pallas_call | solution.py:31
  119.9 1.2 shard_map.165
  121.3 1.3 collective-permute-start.19
  123.4 1.1 collective-permute-start.21
  125.5 2.4 %collective-permute-done.20.a2 = bf16[96,256]{1,0:T(8,128)(2,1)S(1)} collective-permute-done((bf16[96,256]{1,0:T(8,128)(2,1)S(1)}, bf16[96,256]{1,0:T(8,128)(2,1)S(1)}, u32[]{:S(2)}, u32[]{:S(2)}) %collective-permute-start.20) | collective-permute-done | bytes 49184 | tf_op jit(solution)/shard_map/ppermute | solution.py:239
  127.8 1.2 collective-permute-done.21.a3
  129.0 3.9 %output.1 = bf16[96,2048]{1,0:T(8,128)(2,1)} custom-call(s32[4]{0:T(128)S(1)} %add_add_fusion.1.order, bf16[96,256]{1,0:T(8,128)(2,1)S(1)} %get-tuple-element.105.a0, bf16[96,256]{1,0:T(8,128)(2,1)S(1)} %collective-permute-done.19.a1, bf16[96,256]{1,0:T(8,128)(2,1)S(1)} %collective-permute-done.20.a2, bf16[96,256]{1,0:T(8,128)(2,1)S(1)} %collective-permute-done.21.a3, ...), custom_call_target="tpu_custom_call" | custom-call | flops 402653184 | bytes 5242880 | tf_op jit(solution)/shard_map/output/pallas_call | solution.py:343
  (47 shorter events, 7.1 us)
Async XLA Ops:
  0.0 53.4 %collective-permute-start = (bf16[96,2048]{1,0:T(8,128)(2,1)}, bf16[96,2048]{1,0:T(8,128)(2,1)S(1)}, u32[]{:S(2)}, u32[]{:S(2)}) collective-permute-start(bf16[96,2048]{1,0:T(8,128)(2,1)} %bitcast.18), channel_id=1, source_target_pairs={{0,2},{2,4},{4,6},{6,0},{1,3},{3,5},{5,7},{7,1},{8,10},{10,12},{12... | collective-permute-start | bytes 1179656 | tf_op jit(solution)/shard_map/ppermute | solution.py:239
  1.6 51.8 %collective-permute-start.1 = (bf16[96,2048]{1,0:T(8,128)(2,1)}, bf16[96,2048]{1,0:T(8,128)(2,1)}, u32[]{:S(2)}, u32[]{:S(2)}) collective-permute-start(bf16[96,2048]{1,0:T(8,128)(2,1)} %bitcast.19), channel_id=1, source_target_pairs={{0,6},{2,0},{4,2},{6,4},{1,7},{3,1},{5,3},{7,5},{8,14},{10,8},{12,... | collective-permute-start | bytes 1179656 | tf_op jit(solution)/shard_map/ppermute | solution.py:239
  3.2 50.2 %collective-permute-start.2 = (bf16[96,2048]{1,0:T(8,128)(2,1)}, bf16[96,2048]{1,0:T(8,128)(2,1)}, u32[]{:S(2)}, u32[]{:S(2)}) collective-permute-start(bf16[96,2048]{1,0:T(8,128)(2,1)} %bitcast.20), channel_id=1, source_target_pairs={{0,4},{2,6},{4,0},{6,2},{1,5},{3,7},{5,1},{7,3},{8,12},{10,14},{12... | collective-permute-start | bytes 1179656 | tf_op jit(solution)/shard_map/ppermute | solution.py:239
  6.0 0.7 copy-start.3
  8.6 38.8 %all-to-all-start = ((f32[16,4,640]{2,1,0:T(4,128)}), f32[16,4,640]{2,1,0:T(4,128)S(1)}, u32[]{:S(2)}, u32[]{:S(2)}) async-start(f32[16,4,640]{2,1,0:T(4,128)} %modulation.1), calls=%async_computation | async-start | bytes 327680 | tf_op jit(solution)/shard_map/all_to_all | solution.py:283
  33.6 23.3 %copy-start = (bf16[1,96,2048]{2,1,0:T(8,128)(2,1)S(1)}, bf16[1,96,2048]{2,1,0:T(8,128)(2,1)}, u32[]{:S(2)}) copy-start(bf16[1,96,2048]{2,1,0:T(8,128)(2,1)} %param.16) | copy-start | bytes 1179652
  33.6 23.3 %copy-start.2 = (bf16[1,16,2048]{2,1,0:T(8,128)(2,1)S(1)}, bf16[1,16,2048]{2,1,0:T(8,128)(2,1)}, u32[]{:S(2)}) copy-start(bf16[1,16,2048]{2,1,0:T(8,128)(2,1)} %param.18) | copy-start | bytes 196612
  33.6 23.3 %copy-start.4 = (f32[2048]{0:T(1024)S(1)}, f32[2048]{0:T(1024)}, u32[]{:S(2)}) copy-start(f32[2048]{0:T(1024)} %param.23) | copy-start | bytes 24580
  33.6 23.3 %copy-start.5 = (f32[128]{0:T(128)S(1)}, f32[128]{0:T(128)}, u32[]{:S(2)}) copy-start(f32[128]{0:T(128)} %param.28) | copy-start | bytes 1540
  48.1 8.8 %all-to-all-start.1 = ((f32[4,4,640]{2,1,0:T(4,128)}), f32[4,4,640]{2,1,0:T(4,128)S(1)}, u32[]{:S(2)}, u32[]{:S(2)}) async-start(f32[4,4,640]{2,1,0:T(4,128)} %shard_map.154), calls=%async_computation.1 | async-start | bytes 81920 | tf_op jit(solution)/shard_map/all_to_all | solution.py:285
  51.5 11.1 %copy-start.1 = (bf16[2048,256]{1,0:T(8,128)(2,1)S(1)}, bf16[2048,256]{1,0:T(8,128)(2,1)}, u32[]{:S(2)}) copy-start(bf16[2048,256]{1,0:T(8,128)(2,1)} %wq.1) | copy-start | bytes 3145732
  51.5 11.1 %copy-start.6 = (f32[128]{0:T(128)S(1)}, f32[128]{0:T(128)}, u32[]{:S(2)}) copy-start(f32[128]{0:T(128)} %param.27) | copy-start | bytes 1540
  59.2 9.3 %collective-permute-start.3 = (bf16[2,400,128]{2,1,0:T(8,128)(2,1)S(1)}, bf16[2,400,128]{2,1,0:T(8,128)(2,1)S(1)}, u32[]{:S(2)}, u32[]{:S(2)}) collective-permute-start(bf16[2,400,128]{2,1,0:T(8,128)(2,1)S(1)} %get-tuple-element.58.refs_2_), channel_id=1, source_target_pairs={{0,8},{8,16},{16,24},{24,32},{32,40},{40,48},{48,56},{56,64},{64,7... | collective-permute-start | bytes 614408 | tf_op jit(solution)/shard_map/ppermute | solution.py:239
  60.6 7.9 %collective-permute-start.4 = (bf16[2,400,128]{2,1,0:T(8,128)(2,1)S(1)}, bf16[2,400,128]{2,1,0:T(8,128)(2,1)S(1)}, u32[]{:S(2)}, u32[]{:S(2)}) collective-permute-start(bf16[2,400,128]{2,1,0:T(8,128)(2,1)S(1)} %get-tuple-element.58.refs_2_), channel_id=1, source_target_pairs={{0,120},{8,0},{16,8},{24,16},{32,24},{40,32},{48,40},{56,48},{64,5... | collective-permute-start | bytes 614408 | tf_op jit(solution)/shard_map/ppermute | solution.py:239
  68.6 8.3 %collective-permute-start.5 = (bf16[2,400,128]{2,1,0:T(8,128)(2,1)S(1)}, bf16[2,400,128]{2,1,0:T(8,128)(2,1)S(1)}, u32[]{:S(2)}, u32[]{:S(2)}) collective-permute-start(bf16[2,400,128]{2,1,0:T(8,128)(2,1)S(1)} %collective-permute-done.3.refs_2_), channel_id=1, source_target_pairs={{0,8},{8,16},{16,24},{24,32},{32,40},{40,48},{48,56},{56,64},{64,7... | collective-permute-start | bytes 614408 | tf_op jit(solution)/shard_map/ppermute | solution.py:239
  68.6 8.3 %collective-permute-start.6 = (bf16[2,400,128]{2,1,0:T(8,128)(2,1)S(1)}, bf16[2,400,128]{2,1,0:T(8,128)(2,1)S(1)}, u32[]{:S(2)}, u32[]{:S(2)}) collective-permute-start(bf16[2,400,128]{2,1,0:T(8,128)(2,1)S(1)} %collective-permute-done.4.refs_3_), channel_id=1, source_target_pairs={{0,120},{8,0},{16,8},{24,16},{32,24},{40,32},{48,40},{56,48},{64,5... | collective-permute-start | bytes 614408 | tf_op jit(solution)/shard_map/ppermute | solution.py:239
  76.9 7.4 %collective-permute-start.7 = (bf16[2,400,128]{2,1,0:T(8,128)(2,1)S(1)}, bf16[2,400,128]{2,1,0:T(8,128)(2,1)S(1)}, u32[]{:S(2)}, u32[]{:S(2)}) collective-permute-start(bf16[2,400,128]{2,1,0:T(8,128)(2,1)S(1)} %collective-permute-done.5.refs_2_), channel_id=1, source_target_pairs={{0,8},{8,16},{16,24},{24,32},{32,40},{40,48},{48,56},{56,64},{64,7... | collective-permute-start | bytes 614408 | tf_op jit(solution)/shard_map/ppermute | solution.py:239
  76.9 7.4 %collective-permute-start.8 = (bf16[2,400,128]{2,1,0:T(8,128)(2,1)S(1)}, bf16[2,400,128]{2,1,0:T(8,128)(2,1)S(1)}, u32[]{:S(2)}, u32[]{:S(2)}) collective-permute-start(bf16[2,400,128]{2,1,0:T(8,128)(2,1)S(1)} %collective-permute-done.6.refs_3_), channel_id=1, source_target_pairs={{0,120},{8,0},{16,8},{24,16},{32,24},{40,32},{48,40},{56,48},{64,5... | collective-permute-start | bytes 614408 | tf_op jit(solution)/shard_map/ppermute | solution.py:239
  84.3 7.0 %collective-permute-start.9 = (bf16[2,400,128]{2,1,0:T(8,128)(2,1)S(1)}, bf16[2,400,128]{2,1,0:T(8,128)(2,1)S(1)}, u32[]{:S(2)}, u32[]{:S(2)}) collective-permute-start(bf16[2,400,128]{2,1,0:T(8,128)(2,1)S(1)} %collective-permute-done.7.refs_2_), channel_id=1, source_target_pairs={{0,8},{8,16},{16,24},{24,32},{32,40},{40,48},{48,56},{56,64},{64,7... | collective-permute-start | bytes 614408 | tf_op jit(solution)/shard_map/ppermute | solution.py:239
  85.4 5.9 %collective-permute-start.10 = (bf16[2,400,128]{2,1,0:T(8,128)(2,1)S(1)}, bf16[2,400,128]{2,1,0:T(8,128)(2,1)S(1)}, u32[]{:S(2)}, u32[]{:S(2)}) collective-permute-start(bf16[2,400,128]{2,1,0:T(8,128)(2,1)S(1)} %collective-permute-done.8.refs_3_), channel_id=1, source_target_pairs={{0,120},{8,0},{16,8},{24,16},{32,24},{40,32},{48,40},{56,48},{64,5... | collective-permute-start | bytes 614408 | tf_op jit(solution)/shard_map/ppermute | solution.py:239
  91.3 7.0 %collective-permute-start.11 = (bf16[2,400,128]{2,1,0:T(8,128)(2,1)S(1)}, bf16[2,400,128]{2,1,0:T(8,128)(2,1)S(1)}, u32[]{:S(2)}, u32[]{:S(2)}) collective-permute-start(bf16[2,400,128]{2,1,0:T(8,128)(2,1)S(1)} %collective-permute-done.9.refs_2_), channel_id=1, source_target_pairs={{0,8},{8,16},{16,24},{24,32},{32,40},{40,48},{48,56},{56,64},{64,7... | collective-permute-start | bytes 614408 | tf_op jit(solution)/shard_map/ppermute | solution.py:239
  92.6 5.8 %collective-permute-start.12 = (bf16[2,400,128]{2,1,0:T(8,128)(2,1)S(1)}, bf16[2,400,128]{2,1,0:T(8,128)(2,1)S(1)}, u32[]{:S(2)}, u32[]{:S(2)}) collective-permute-start(bf16[2,400,128]{2,1,0:T(8,128)(2,1)S(1)} %collective-permute-done.10.refs_3_), channel_id=1, source_target_pairs={{0,120},{8,0},{16,8},{24,16},{32,24},{40,32},{48,40},{56,48},{64,5... | collective-permute-start | bytes 614408 | tf_op jit(solution)/shard_map/ppermute | solution.py:239
  98.4 7.0 %collective-permute-start.13 = (bf16[2,400,128]{2,1,0:T(8,128)(2,1)S(1)}, bf16[2,400,128]{2,1,0:T(8,128)(2,1)S(1)}, u32[]{:S(2)}, u32[]{:S(2)}) collective-permute-start(bf16[2,400,128]{2,1,0:T(8,128)(2,1)S(1)} %collective-permute-done.11.refs_2_), channel_id=1, source_target_pairs={{0,8},{8,16},{16,24},{24,32},{32,40},{40,48},{48,56},{56,64},{64,7... | collective-permute-start | bytes 614408 | tf_op jit(solution)/shard_map/ppermute | solution.py:239
  99.9 5.8 %collective-permute-start.14 = (bf16[2,400,128]{2,1,0:T(8,128)(2,1)S(1)}, bf16[2,400,128]{2,1,0:T(8,128)(2,1)S(1)}, u32[]{:S(2)}, u32[]{:S(2)}) collective-permute-start(bf16[2,400,128]{2,1,0:T(8,128)(2,1)S(1)} %collective-permute-done.12.refs_3_), channel_id=1, source_target_pairs={{0,120},{8,0},{16,8},{24,16},{32,24},{40,32},{48,40},{56,48},{64,5... | collective-permute-start | bytes 614408 | tf_op jit(solution)/shard_map/ppermute | solution.py:239
  103.9 20.7 %copy-start.7 = (f32[1024]{0:T(1024)S(1)}, f32[1024]{0:T(1024)}, u32[]{:S(2)}) copy-start(f32[1024]{0:T(1024)} %param.30) | copy-start | bytes 12292
  105.7 7.0 %collective-permute-start.15 = (bf16[2,400,128]{2,1,0:T(8,128)(2,1)S(1)}, bf16[2,400,128]{2,1,0:T(8,128)(2,1)S(1)}, u32[]{:S(2)}, u32[]{:S(2)}) collective-permute-start(bf16[2,400,128]{2,1,0:T(8,128)(2,1)S(1)} %collective-permute-done.13.refs_2_), channel_id=1, source_target_pairs={{0,8},{8,16},{16,24},{24,32},{32,40},{40,48},{48,56},{56,64},{64,7... | collective-permute-start | bytes 614408 | tf_op jit(solution)/shard_map/ppermute | solution.py:239
  107.7 5.8 %collective-permute-start.16 = (bf16[2,400,128]{2,1,0:T(8,128)(2,1)S(1)}, bf16[2,400,128]{2,1,0:T(8,128)(2,1)S(1)}, u32[]{:S(2)}, u32[]{:S(2)}) collective-permute-start(bf16[2,400,128]{2,1,0:T(8,128)(2,1)S(1)} %collective-permute-done.14.refs_3_), channel_id=1, source_target_pairs={{0,120},{8,0},{16,8},{24,16},{32,24},{40,32},{48,40},{56,48},{64,5... | collective-permute-start | bytes 614408 | tf_op jit(solution)/shard_map/ppermute | solution.py:239
  113.5 6.0 %collective-permute-start.17 = (bf16[400,128]{1,0:T(8,128)(2,1)S(1)}, bf16[400,128]{1,0:T(8,128)(2,1)S(1)}, u32[]{:S(2)}, u32[]{:S(2)}) collective-permute-start(bf16[400,128]{1,0:T(8,128)(2,1)S(1)} %slice_bitcast_fusion.1), channel_id=1, source_target_pairs={{0,8},{8,16},{16,24},{24,32},{32,40},{40,48},{48,56},{56,64},{64,7... | collective-permute-start | bytes 307208 | tf_op jit(solution)/shard_map/ppermute | solution.py:239
  115.1 4.8 %collective-permute-start.18 = (bf16[400,128]{1,0:T(8,128)(2,1)S(1)}, bf16[400,128]{1,0:T(8,128)(2,1)S(1)}, u32[]{:S(2)}, u32[]{:S(2)}) collective-permute-start(bf16[400,128]{1,0:T(8,128)(2,1)S(1)} %slice_bitcast_fusion), channel_id=1, source_target_pairs={{0,120},{8,0},{16,8},{24,16},{32,24},{40,32},{48,40},{56,48},{64,5... | collective-permute-start | bytes 307208 | tf_op jit(solution)/shard_map/ppermute | solution.py:239
  121.3 4.2 %collective-permute-start.19 = (bf16[96,256]{1,0:T(8,128)(2,1)S(1)}, bf16[96,256]{1,0:T(8,128)(2,1)S(1)}, u32[]{:S(2)}, u32[]{:S(2)}) collective-permute-start(bf16[96,256]{1,0:T(8,128)(2,1)S(1)} %get-tuple-element.106), channel_id=1, source_target_pairs={{0,6},{2,0},{4,2},{6,4},{1,7},{3,1},{5,3},{7,5},{8,14},{10,8},{12,... | collective-permute-start | bytes 147464 | tf_op jit(solution)/shard_map/ppermute | solution.py:239
  122.5 5.3 %collective-permute-start.20 = (bf16[96,256]{1,0:T(8,128)(2,1)S(1)}, bf16[96,256]{1,0:T(8,128)(2,1)S(1)}, u32[]{:S(2)}, u32[]{:S(2)}) collective-permute-start(bf16[96,256]{1,0:T(8,128)(2,1)S(1)} %get-tuple-element.107), channel_id=1, source_target_pairs={{0,2},{2,4},{4,6},{6,0},{1,3},{3,5},{5,7},{7,1},{8,10},{10,12},{12... | collective-permute-start | bytes 147464 | tf_op jit(solution)/shard_map/ppermute | solution.py:239
  123.4 5.6 %collective-permute-start.21 = (bf16[96,256]{1,0:T(8,128)(2,1)S(1)}, bf16[96,256]{1,0:T(8,128)(2,1)S(1)}, u32[]{:S(2)}, u32[]{:S(2)}) collective-permute-start(bf16[96,256]{1,0:T(8,128)(2,1)S(1)} %get-tuple-element.108), channel_id=1, source_target_pairs={{0,4},{2,6},{4,0},{6,2},{1,5},{3,7},{5,1},{7,3},{8,12},{10,14},{12... | collective-permute-start | bytes 147464 | tf_op jit(solution)/shard_map/ppermute | solution.py:239
where the time goes:
time: 133 us
  starting transfers between devices  62.1 us (47%)
  waiting for transfers between devices  33.6 us (25%)
  Pallas kernels  28.6 us (22%)
  other arithmetic  6.66 us (5%)
  local copies, waits for them, and re-layouts  1.61 us (1%)
    ppermute x22, starting transfers between devices, shifted(): return lax.ppermute(x, axis, [(i, (i + by) % count) for i in range(count)])  34.8 us
    all_to_all x1, starting transfers between devices, on_device(): parts = lax.all_to_all(parts, 'sp', 0, 0)  24 us
    pallas_call x13, Pallas kernels, run(): pl.pallas_call(body, out_shape=outs if single else tuple(shapes), in_spec...  22.8 us
    ppermute x22, waiting for transfers between devices, shifted(): return lax.ppermute(x, axis, [(i, (i + by) % count) for i in range(count)])  20.2 us
    all_to_all x1, waiting for transfers between devices, on_device(): parts = lax.all_to_all(parts, 'sp', 0, 0)  10 us
    pallas_call x1, Pallas kernels, on_device(): pl.pallas_call(out_kernel, out_shape=shape((own_rows, width), BF16), in_s...  3.87 us
    all_to_all x1, waiting for transfers between devices, on_device(): mod = lax.all_to_all(mod, 'tp', 0, 0)  3.43 us
    all_to_all x1, starting transfers between devices, on_device(): mod = lax.all_to_all(mod, 'tp', 0, 0)  3.36 us
  transfers between devices with their start and end apart: 24, of which 18 were waited for; matrix products, arithmetic and copies ran while one was open for 6% of the time, Pallas kernels for 16%

commit v1 on v0

--- a/solution.py
+++ b/solution.py
@@ -20,7 +20,7 @@
 MIB = 1 << 20
 
 
-def local_call(body, outs, *, flops, limit=12, scratch=(), aliases=None):
+def local_call(body, outs, *, flops, limit=12, scratch=(), aliases=None, specs=None):
     single = not isinstance(outs, (tuple, list))
     shapes = [outs] if single else list(outs)
     space = pl.BlockSpec(memory_space=pltpu.VMEM)
@@ -31,7 +31,7 @@
         return pl.pallas_call(
             body,
             out_shape=outs if single else tuple(shapes),
-            in_specs=[space] * len(args),
+            in_specs=specs or [space] * len(args),
             out_specs=space if single else tuple([space] * len(shapes)),
             scratch_shapes=list(scratch),
             input_output_aliases=aliases or {},
@@ -55,15 +55,25 @@
     return jax.ShapeDtypeStruct(dims, dtype)
 
 
-def modulation_kernel(cond, cond_ctx, wa, wb, wc, out_ref, weights, sem):
+def modulation_kernel(
+    cond, cond_ctx, wa, wb, wc, out_ref, weights, own_ref, ctx_ref, rows_ref, sem
+):
     copies = [
-        pltpu.make_async_copy(w, weights.at[i], sem.at[i]) for i, w in enumerate((wa, wb, wc))
+        pltpu.make_async_copy(source, target, sem.at[i])
+        for i, (source, target) in enumerate(
+            ((cond, own_ref), (cond_ctx, ctx_ref))
+            + tuple((w, weights.at[i]) for i, w in enumerate((wa, wb, wc)))
+        )
     ]
     for copy in copies:
         copy.start()
+    copies.pop(0).wait()
+    copies.pop(0).wait()
     depth = weights.shape[1]
     at = pl.ds(pl.multiple_of(lax.axis_index("sp") * depth, depth), depth)
-    rows = jnp.concatenate([cond[:, at].astype(F32), cond_ctx[:, at].astype(F32)], 0)
+    rows_ref[0:1, :] = own_ref[...].astype(F32)
+    rows_ref[1:2, :] = ctx_ref[...].astype(F32).reshape(1, -1)
+    rows = rows_ref[:, at]
     acted = (rows * jax.nn.sigmoid(rows)).astype(BF16)
     for copy in copies:
         copy.wait()
@@ -79,18 +89,21 @@
 
 
 def sum_kernel(parts, out_ref):
-    total = jnp.sum(parts[...], 0)
-    for i in range(out_ref.shape[0]):
-        out_ref[i] = total
+    out_ref[...] = jnp.sum(parts[...], 0)
 
 
 def kv_kernel(
-    x0, x1, x2, x3, ctx, mod, gain, wkv, key_gain, cosine, sine, chunk_ref, normed_ref
+    owners, x0, x1, x2, x3, ctx, m0, m1, m2, m3, gain, wkv, key_gain, cosine, sine,
+    chunk_ref, normed_ref, gate_ref, mod_ref,
 ):
-    wide = gain.shape[1] // mod.shape[0]
+    for i, mod in enumerate((m0, m1, m2, m3)):
+        wide = gain.shape[1] // 4
+        at = pl.ds(pl.multiple_of(owners[i] * wide, wide), wide)
+        mod_ref[:, at] = mod[:, :wide]
+        gate_ref[:, at] = jnp.concatenate([mod[r : r + 1, wide:] for r in range(4)], 1)
 
     def row_of(index):
-        return jnp.concatenate([mod[b, index : index + 1, :wide] for b in range(mod.shape[0])], 1)
+        return mod_ref[index : index + 1, :]
 
     gains = gain[...]
     amp, shift = gains * (1.0 + row_of(1)), row_of(0)
@@ -155,8 +168,11 @@
         acc_in, stat_in, acc_out, stat_out = rest
     total = qt.shape[1]
     width = 256
-    for begin in range(0, total, width):
-        part = slice(begin, begin + width)
+
+
+    @pl.loop(0, total // width)
+    def _(block):
+        part = pl.ds(pl.multiple_of(block * width, width), width)
         q = qt[:, part]
         bias = lift[:, part]
         if first:
@@ -185,6 +201,14 @@
         stat_out[1:2, part] = low
 
 
+def keeping(body, source, *refs):
+    *refs, kept, sem = refs
+    load = pltpu.make_async_copy(source, kept, sem)
+    load.start()
+    body(*refs)
+    load.wait()
+
+
 def finish_kernel(acc, stat, *targets):
     own = targets[0].shape[0]
     rows = len(targets) * own
@@ -195,15 +219,8 @@
             target[:, h * HEAD_DIM : (h + 1) * HEAD_DIM] = att[b * own : (b + 1) * own]
 
 
-def out_kernel(order, a0, a1, a2, a3, gain, w_out, latent, mod, out_ref, weights, sem):
-    blocks = mod.shape[0]
-    wide = out_ref.shape[1] // blocks
-    copies = [
-        pltpu.make_async_copy(w_out.at[:, pl.ds(b * wide, wide)], weights.at[b], sem.at[b])
-        for b in range(blocks)
-    ]
-    for copy in copies:
-        copy.start()
+def out_kernel(order, a0, a1, a2, a3, gain, w_out, latent, gate, out_ref):
+    wide = 512
     cols = a0.shape[1]
     atts = [a[...].astype(F32) for a in (a0, a1, a2, a3)]
     total = sum(jnp.sum(a * a, -1, keepdims=True) for a in atts)
@@ -211,15 +228,13 @@
     normed = [
         (a * scale * gain[pl.ds(order[i], 1), :]).astype(BF16) for i, a in enumerate(atts)
     ]
-    for b in range(blocks):
-        copies[b].wait()
-        part = slice(b * wide, (b + 1) * wide)
+    for begin in range(0, out_ref.shape[1], wide):
+        part = slice(begin, begin + wide)
         mix = 0.0
         for i, a in enumerate(normed):
             at = pl.multiple_of(order[i] * cols, cols)
-            mix += jnp.dot(a, weights[b, pl.ds(at, cols), :], preferred_element_type=F32)
-        gate = jnp.concatenate([mod[b, r : r + 1, wide:] for r in range(mod.shape[1])], 1)
-        out = latent[:, part].astype(F32) + gate * mix
+            mix += jnp.dot(a, w_out[pl.ds(at, cols), part], preferred_element_type=F32)
+        out = latent[:, part].astype(F32) + gate[:, part] * mix
         out_ref[:, part] = out.astype(BF16)
 
 
@@ -270,34 +285,43 @@
     parts = pl.pallas_call(
         modulation_kernel,
         out_shape=shape((n_sp, *packed), F32),
-        in_specs=[space, space, FAR, FAR, FAR],
+        in_specs=[FAR] * 5,
         out_specs=space,
         scratch_shapes=[
             pltpu.VMEM((3, in_rows, out_cols), BF16),
-            pltpu.SemaphoreType.DMA((3,)),
+            pltpu.VMEM((1, width), BF16),
+            pltpu.VMEM((width,), BF16),
+            pltpu.VMEM((2, width), F32),
+            pltpu.SemaphoreType.DMA((5,)),
         ],
         compiler_params=pltpu.CompilerParams(vmem_limit_bytes=4 * MIB),
         cost_estimate=pl.CostEstimate(flops=10**6, bytes_accessed=MIB, transcendentals=0),
         name="modulation",
-    )(cond, cond_ctx[None], far(w_shift), far(w_scale), far(w_gate))
+    )(far(cond), far(cond_ctx), far(w_shift), far(w_scale), far(w_gate))
     parts = lax.all_to_all(parts, "sp", 0, 0)
-    mod = local_call(sum_kernel, shape((n_tp, *packed), F32), flops=10**6, limit=4)(parts)
-    mod = lax.all_to_all(mod, "tp", 0, 0)
+    summed = local_call(sum_kernel, shape(packed, F32), flops=10**6, limit=4)(parts)
+    mods = [summed] + [shifted(summed, "tp", by) for by in (1, -1, 2)]
 
     latents = [latent]
     for by in (1, -1, 2):
         latents.append(shifted(latent, "tp", by))
-    owners = jnp.stack([tp, (tp - 1) % n_tp, (tp + 1) % n_tp, (tp + 2) % n_tp])
+    owners = jnp.stack([tp, (tp - 1) % n_tp, (tp + 1) % n_tp, (tp + 2) % n_tp]).astype(jnp.int32)
     positions = sp * rows + (owners[:, None] * own_rows + jnp.arange(own_rows)[None]).reshape(-1)
     cosine, sine = angles(positions.astype(jnp.int32))
     wkv = jnp.concatenate([w_key, w_value], 1)
     length = ctx_rows + rows
-    chunk, normed = local_call(
+    chunk, normed, gate = local_call(
         kv_kernel,
-        (shape((2, length, HEAD_DIM), BF16), shape((length, width), BF16)),
+        (
+            shape((2, length, HEAD_DIM), BF16),
+            shape((length, width), BF16),
+            shape((1, width), F32),
+        ),
         flops=2 * length * width * 256,
         limit=16,
-    )(*latents, context, mod, norm_gain[None], wkv, key_gain[None], cosine, sine)
+        specs=[pl.BlockSpec(memory_space=pltpu.SMEM)] + [space] * 14,
+        scratch=[pltpu.VMEM((4, width), F32)],
+    )(owners, *latents, context, *mods, norm_gain[None], wkv, key_gain[None], cosine, sine)
     q_cols = w_query.shape[1]
     group = q_cols // HEAD_DIM
     qt = local_call(
@@ -305,6 +329,10 @@
     )(normed, w_query, query_gain[None], cosine, sine)
     lift = (ctx_lift + math.log(rows / ctx_rows)) / FACTOR
     lift = jnp.repeat(lift, rows)[None]
+
+    order = jnp.stack([tp, (tp + 1) % n_tp, (tp - 1) % n_tp, (tp + 2) % n_tp]).astype(jnp.int32)
+    gain_rows = out_gain.reshape(n_tp, q_cols)
+    order, gain_rows, lift, chunk = lax.optimization_barrier((order, gain_rows, lift, chunk))
 
     lanes = group * rows
     state_shapes = (shape((HEAD_DIM, lanes), F32), shape((2, lanes), F32))
@@ -324,37 +352,39 @@
             aliases={len(given) - 2: 0, len(given) - 1: 1},
         )(*given)
 
+    def hop(x, by, state):
+        x, state = lax.optimization_barrier((x, state))
+        return x, shifted(x, "sp", by), state
+
     right, left = shifted(chunk, "sp", 1), shifted(chunk, "sp", -1)
     for _ in range(n_sp // 2 - 2):
-        right, left, state = lax.optimization_barrier((right, left, state))
-        arrived = right, left
-        right, left = shifted(right, "sp", 1), shifted(left, "sp", -1)
-        state = attend(state, *arrived)
-    right, left, state = lax.optimization_barrier((right, left, state))
-    last_k, last_v = shifted(right[0], "sp", 1), shifted(left[1], "sp", -1)
-    state = attend(state, right, left)
+        here_right, right, state = hop(right, 1, state)
+        here_left, left, state = hop(left, -1, state)
+        state = attend(state, here_right, here_left)
+    right, state = lax.optimization_barrier((right, state))
+    last_k = shifted(right[0], "sp", 1)
+    left, state = lax.optimization_barrier((left, state))
+    last_v = shifted(left[1], "sp", -1)
+    *state, w_kept = local_call(
+        functools.partial(keeping, functools.partial(attend_kernel, ctx_rows, False, False)),
+        (*state_shapes, pltpu.VMEM(w_out.shape, BF16)),
+        flops=8 * length * lanes * HEAD_DIM,
+        specs=[FAR] + [space] * 6,
+        scratch=[pltpu.SemaphoreType.DMA],
+        aliases={5: 0, 6: 1},
+    )(far(w_out), qt, lift, right, left, *state)
     state = attend(state, last_k, last_v, pairs=True)
 
     own, to_left, to_right, to_far = local_call(
         finish_kernel, [shape((own_rows, q_cols), BF16)] * n_tp, flops=10**6
     )(*state)
     atts = [own, shifted(to_left, "tp", -1), shifted(to_right, "tp", 1), shifted(to_far, "tp", 2)]
-    order = jnp.stack([tp, (tp + 1) % n_tp, (tp - 1) % n_tp, (tp + 2) % n_tp]).astype(jnp.int32)
-    result = pl.pallas_call(
+    result = local_call(
         out_kernel,
-        out_shape=shape((own_rows, width), BF16),
-        in_specs=[pl.BlockSpec(memory_space=pltpu.SMEM)] + [space] * 5 + [FAR, space, space],
-        out_specs=space,
-        scratch_shapes=[
-            pltpu.VMEM((n_tp, w_out.shape[0], out_cols), BF16),
-            pltpu.SemaphoreType.DMA((n_tp,)),
-        ],
-        compiler_params=pltpu.CompilerParams(vmem_limit_bytes=12 * MIB),
-        cost_estimate=pl.CostEstimate(
-            flops=2 * own_rows * width * HEADS * HEAD_DIM, bytes_accessed=5 * MIB, transcendentals=0
-        ),
-        name="output",
-    )(order, *atts, out_gain.reshape(n_tp, q_cols), far(w_out), latent, mod)
+        shape((own_rows, width), BF16),
+        flops=2 * own_rows * width * HEADS * HEAD_DIM,
+        specs=[pl.BlockSpec(memory_space=pltpu.SMEM)] + [space] * 8,
+    )(order, *atts, gain_rows, w_kept, latent, gate)
     return result[None]
 
 

time: 133 us -> 132 us (level)
  other arithmetic: 6.66 us -> 2.19 us
  waiting for transfers between devices: 33.6 us -> 36.8 us
  local copies, waits for them, and re-layouts: 1.61 us -> 0.24 us
    ppermute x22 -> x25, starting transfers between devices: 34.8 us -> 39.4 us  [shifted(): return lax.ppermute(x, axis, [(i, (i + by) % count) for i in range(count)])]
    ppermute x22 -> x25, waiting for transfers between devices: 20.2 us -> 24.5 us  [shifted(): return lax.ppermute(x, axis, [(i, (i + by) % count) for i in range(count)])]
    pallas_call x13 -> x14, Pallas kernels: 22.8 us -> 26.7 us  [run(): pl.pallas_call(body, out_shape=outs if single else tuple(shapes), in_spec...]
    pallas_call x1 -> x0, Pallas kernels: 3.87 us -> none  [on_device(): pl.pallas_call(out_kernel, out_shape=shape((own_rows, width), BF16), in_s...]
    all_to_all x1 -> x0, waiting for transfers between devices: 3.43 us -> none  [on_device(): mod = lax.all_to_all(mod, 'tp', 0, 0)]
    all_to_all x1 -> x0, starting transfers between devices: 3.36 us -> none  [on_device(): mod = lax.all_to_all(mod, 'tp', 0, 0)]
    all_to_all x1, waiting for transfers between devices: 10 us -> 12.3 us  [on_device(): parts = lax.all_to_all(parts, 'sp', 0, 0)]
    concatenate x1, other arithmetic: 1.9 us -> 0.37 us  [angles(): return (jnp.concatenate(cosine, 1), jnp.concatenate(sine, 1))]
  transfers between devices with their start and end apart: 24 -> 26, of which waited for: 18 -> 15; matrix products, arithmetic and copies ran while one was open for 6% -> 2% of each run, Pallas kernels for 16% -> 17%
where the time goes in v1:
time: 132 us
  starting transfers between devices  63.4 us (48%)
  waiting for transfers between devices  36.8 us (28%)
  Pallas kernels  28.7 us (22%)
  other arithmetic  2.19 us (2%)
    ppermute x25, starting transfers between devices, shifted(): return lax.ppermute(x, axis, [(i, (i + by) % count) for i in range(count)])  39.4 us
    pallas_call x14, Pallas kernels, run(): pl.pallas_call(body, out_shape=outs if single else tuple(shapes), in_spec...  26.7 us
    ppermute x25, waiting for transfers between devices, shifted(): return lax.ppermute(x, axis, [(i, (i + by) % count) for i in range(count)])  24.5 us
    all_to_all x1, starting transfers between devices, on_device(): parts = lax.all_to_all(parts, 'sp', 0, 0)  24 us
    all_to_all x1, waiting for transfers between devices, on_device(): parts = lax.all_to_all(parts, 'sp', 0, 0)  12.3 us
  transfers between devices with their start and end apart: 26, of which 15 were waited for; matrix products, arithmetic and copies ran while one was open for 2% of the time, Pallas kernels for 17%

profile of v1, /device:TPU:40, one launch (start us, length us, event | category | flops | bytes accessed | tf_op | source)
XLA Modules:
  0.0 131.7 jit_solution(2638296525217596181)
XLA Ops:
  0.0 1.6 %collective-permute-start = (bf16[96,2048]{1,0:T(8,128)(2,1)}, bf16[96,2048]{1,0:T(8,128)(2,1)S(1)}, u32[]{:S(2)}, u32[]{:S(2)}) collective-permute-start(bf16[96,2048]{1,0:T(8,128)(2,1)} %bitcast.18), channel_id=1, source_target_pairs={{0,2},{2,4},{4,6},{6,0},{1,3},{3,5},{5,7},{7,1},{8,10},{10,12},{12... | collective-permute-start | bytes 1179656 | tf_op jit(solution)/shard_map/ppermute | solution.py:254
  1.6 1.6 %collective-permute-start.1 = (bf16[96,2048]{1,0:T(8,128)(2,1)}, bf16[96,2048]{1,0:T(8,128)(2,1)}, u32[]{:S(2)}, u32[]{:S(2)}) collective-permute-start(bf16[96,2048]{1,0:T(8,128)(2,1)} %bitcast.19), channel_id=1, source_target_pairs={{0,6},{2,0},{4,2},{6,4},{1,7},{3,1},{5,3},{7,5},{8,14},{10,8},{12,... | collective-permute-start | bytes 1179656 | tf_op jit(solution)/shard_map/ppermute | solution.py:254
  3.3 2.0 %collective-permute-start.2 = (bf16[96,2048]{1,0:T(8,128)(2,1)}, bf16[96,2048]{1,0:T(8,128)(2,1)}, u32[]{:S(2)}, u32[]{:S(2)}) collective-permute-start(bf16[96,2048]{1,0:T(8,128)(2,1)} %bitcast.20), channel_id=1, source_target_pairs={{0,4},{2,6},{4,0},{6,2},{1,5},{3,7},{5,1},{7,3},{8,12},{10,14},{12... | collective-permute-start | bytes 1179656 | tf_op jit(solution)/shard_map/ppermute | solution.py:254
  5.3 1.9 %modulation.1 = f32[16,4,640]{2,1,0:T(4,128)} custom-call(bf16[1,2048]{1,0:T(2,128)(2,1)} %cond.1, bf16[2048]{0:T(1024)(128)(2,1)} %cond_ctx.1, bf16[128,512]{1,0:T(8,128)(2,1)} %wa.1, bf16[128,512]{1,0:T(8,128)(2,1)} %wb.1, bf16[128,512]{1,0:T(8,128)(2,1)} %wc.1), custom_call_target="tpu_custom_call" | custom-call | flops 1000000 | bytes 1048576 | tf_op jit(solution)/shard_map/modulation/pallas_call | solution.py:285
  7.3 24.0 %all-to-all-start = ((f32[16,4,640]{2,1,0:T(4,128)}), f32[16,4,640]{2,1,0:T(4,128)S(1)}, u32[]{:S(2)}, u32[]{:S(2)}) async-start(f32[16,4,640]{2,1,0:T(4,128)} %modulation.1), calls=%async_computation | async-start | bytes 327680 | tf_op jit(solution)/shard_map/all_to_all | solution.py:301
  31.6 1.4 %fusion = (f32[384,32]{1,0:T(8,128)S(1)}, f32[384,32]{1,0:T(8,128)S(1)}, f32[384,32]{1,0:T(8,128)S(1)}, f32[384,32]{1,0:T(8,128)S(1)}, f32[384,32]{1,0:T(8,128)S(1)}, /*index=5*/f32[384,32]{1,0:T(8,128)S(1)}) fusion(f32[32]{0:T(128)S(1)} %multiply_power_fusion, f32[384]{0:T(512)S(1)} %get-tuple-element.157, f32[384]{0:T(512)S(1)} %get-tuple-element.158), kind=kLoop, calls=%fused_computation.9 | loop fusion | flops 49152 | bytes 298112 | tf_op jit(solution)/shard_map/neg | solution.py:248
  33.2 0.4 pad_maximum_fusion.1
  33.8 12.3 %all-to-all-done.parts = f32[16,4,640]{2,1,0:T(4,128)S(1)} async-done(((f32[16,4,640]{2,1,0:T(4,128)}), f32[16,4,640]{2,1,0:T(4,128)S(1)}, u32[]{:S(2)}, u32[]{:S(2)}) %all-to-all-start) | async-done | bytes 163872 | tf_op jit(solution)/shard_map/all_to_all | solution.py:301
  46.1 0.8 collective-permute-start.3
  47.0 2.5 %collective-permute-start.4 = (f32[4,640]{1,0:T(4,128)S(1)}, f32[4,640]{1,0:T(4,128)S(1)}, u32[]{:S(2)}, u32[]{:S(2)}) collective-permute-start(f32[4,640]{1,0:T(4,128)S(1)} %shard_map.154.m0), channel_id=1, source_target_pairs={{0,6},{2,0},{4,2},{6,4},{1,7},{3,1},{5,3},{7,5},{8,14},{10,8},{12,... | collective-permute-start | bytes 30728 | tf_op jit(solution)/shard_map/ppermute | solution.py:254
  49.5 0.3 collective-permute-start.5
  49.9 1.2 collective-permute-done.3.m1
  51.1 3.5 %collective-permute-done.5.m3 = f32[4,640]{1,0:T(4,128)S(1)} collective-permute-done((f32[4,640]{1,0:T(4,128)S(1)}, f32[4,640]{1,0:T(4,128)S(1)}, u32[]{:S(2)}, u32[]{:S(2)}) %collective-permute-start.5) | collective-permute-done | bytes 10272 | tf_op jit(solution)/shard_map/ppermute | solution.py:254
  54.7 2.3 %shard_map.155 = (bf16[2,400,128]{2,1,0:T(8,128)(2,1)S(1)}, bf16[400,2048]{1,0:T(8,128)(2,1)S(1)}, f32[1,2048]{1,0:T(1,128)S(1)}) custom-call(s32[4]{0:T(128)S(1)} %get-tuple-element.150.owners, bf16[96,2048]{1,0:T(8,128)(2,1)S(1)} %bitcast.21, bf16[96,2048]{1,0:T(8,128)(2,1)S(1)} %collective-permute-done.x1, bf16[96,2048]{1,0:T(8,128)(2,1)} %collective-permute-done.1.x2, ...), custom_call_target="tpu_custom_call" | custom-call | flops 419430400 | bytes 4981264 | tf_op jit(solution)/shard_map/pallas_call | solution.py:31
  57.0 1.5 %collective-permute-start.6 = (bf16[2,400,128]{2,1,0:T(8,128)(2,1)S(1)}, bf16[2,400,128]{2,1,0:T(8,128)(2,1)S(1)}, u32[]{:S(2)}, u32[]{:S(2)}) collective-permute-start(bf16[2,400,128]{2,1,0:T(8,128)(2,1)S(1)} %get-tuple-element.81.refs_2_), channel_id=1, source_target_pairs={{0,8},{8,16},{16,24},{24,32},{32,40},{40,48},{48,56},{56,64},{64,7... | collective-permute-start | bytes 614408 | tf_op jit(solution)/shard_map/ppermute | solution.py:254
  58.5 1.9 %collective-permute-start.8 = (bf16[2,400,128]{2,1,0:T(8,128)(2,1)S(1)}, bf16[2,400,128]{2,1,0:T(8,128)(2,1)S(1)}, u32[]{:S(2)}, u32[]{:S(2)}) collective-permute-start(bf16[2,400,128]{2,1,0:T(8,128)(2,1)S(1)} %get-tuple-element.81.refs_2_), channel_id=1, source_target_pairs={{0,120},{8,0},{16,8},{24,16},{32,24},{40,32},{48,40},{56,48},{64,5... | collective-permute-start | bytes 614408 | tf_op jit(solution)/shard_map/ppermute | solution.py:254
  60.4 1.1 shard_map.156.refs_0_
  61.5 1.5 %shard_map.157 = (f32[128,768]{1,0:T(8,128)S(1)}, f32[2,768]{1,0:T(2,128)S(1)}) custom-call(bf16[128,768]{1,0:T(8,128)(2,1)S(1)} %shard_map.156.refs_0_, f32[1,768]{1,0:T(1,128)S(1)} %bitcast.24, bf16[2,400,128]{2,1,0:T(8,128)(2,1)S(1)} %get-tuple-element.81.refs_2_), custom_call_target="tpu_custom_call" | custom-call | flops 157286400 | bytes 803840 | tf_op jit(solution)/shard_map/pallas_call | solution.py:31
  63.0 2.6 %collective-permute-done.6.refs_2_ = bf16[2,400,128]{2,1,0:T(8,128)(2,1)S(1)} collective-permute-done((bf16[2,400,128]{2,1,0:T(8,128)(2,1)S(1)}, bf16[2,400,128]{2,1,0:T(8,128)(2,1)S(1)}, u32[]{:S(2)}, u32[]{:S(2)}) %collective-permute-start.6) | collective-permute-done | bytes 204832 | tf_op jit(solution)/shard_map/ppermute | solution.py:254
  65.6 3.2 %collective-permute-start.10 = (bf16[2,400,128]{2,1,0:T(8,128)(2,1)S(1)}, bf16[2,400,128]{2,1,0:T(8,128)(2,1)S(1)}, u32[]{:S(2)}, u32[]{:S(2)}) collective-permute-start(bf16[2,400,128]{2,1,0:T(8,128)(2,1)S(1)} %collective-permute-done.8.refs_3_), channel_id=1, source_target_pairs={{0,120},{8,0},{16,8},{24,16},{32,24},{40,32},{48,40},{56,48},{64,5... | collective-permute-start | bytes 614408 | tf_op jit(solution)/shard_map/ppermute | solution.py:254
  68.9 2.6 %shard_map.158 = (f32[128,768]{1,0:T(8,128)S(1)}, f32[2,768]{1,0:T(2,128)S(1)}) custom-call(bf16[128,768]{1,0:T(8,128)(2,1)S(1)} %shard_map.156.refs_0_, f32[1,768]{1,0:T(1,128)S(1)} %bitcast.25, bf16[2,400,128]{2,1,0:T(8,128)(2,1)S(1)} %collective-permute-done.6.refs_2_, ...), custom_call_target="tpu_custom_call", output_to_operand_aliasing={{0}: (4, {}), {1}: (5, {})} | custom-call | flops 314572800 | bytes 1408000 | tf_op jit(solution)/shard_map/pallas_call | solution.py:31
  71.4 1.8 %collective-permute-done.7.refs_2_ = bf16[2,400,128]{2,1,0:T(8,128)(2,1)S(1)} collective-permute-done((bf16[2,400,128]{2,1,0:T(8,128)(2,1)S(1)}, bf16[2,400,128]{2,1,0:T(8,128)(2,1)S(1)}, u32[]{:S(2)}, u32[]{:S(2)}) %collective-permute-start.7) | collective-permute-done | bytes 204832 | tf_op jit(solution)/shard_map/ppermute | solution.py:254
  73.3 3.2 %collective-permute-start.12 = (bf16[2,400,128]{2,1,0:T(8,128)(2,1)S(1)}, bf16[2,400,128]{2,1,0:T(8,128)(2,1)S(1)}, u32[]{:S(2)}, u32[]{:S(2)}) collective-permute-start(bf16[2,400,128]{2,1,0:T(8,128)(2,1)S(1)} %collective-permute-done.10.refs_3_), channel_id=1, source_target_pairs={{0,120},{8,0},{16,8},{24,16},{32,24},{40,32},{48,40},{56,48},{64,5... | collective-permute-start | bytes 614408 | tf_op jit(solution)/shard_map/ppermute | solution.py:254
  76.5 2.6 %shard_map.159 = (f32[128,768]{1,0:T(8,128)S(1)}, f32[2,768]{1,0:T(2,128)S(1)}) custom-call(bf16[128,768]{1,0:T(8,128)(2,1)S(1)} %shard_map.156.refs_0_, f32[1,768]{1,0:T(1,128)S(1)} %bitcast.26, bf16[2,400,128]{2,1,0:T(8,128)(2,1)S(1)} %collective-permute-done.7.refs_2_, ...), custom_call_target="tpu_custom_call", output_to_operand_aliasing={{0}: (4, {}), {1}: (5, {})} | custom-call | flops 314572800 | bytes 1408000 | tf_op jit(solution)/shard_map/pallas_call | solution.py:31
  79.1 1.2 collective-permute-done.9.refs_2_
  80.2 3.2 %collective-permute-start.14 = (bf16[2,400,128]{2,1,0:T(8,128)(2,1)S(1)}, bf16[2,400,128]{2,1,0:T(8,128)(2,1)S(1)}, u32[]{:S(2)}, u32[]{:S(2)}) collective-permute-start(bf16[2,400,128]{2,1,0:T(8,128)(2,1)S(1)} %collective-permute-done.12.refs_3_), channel_id=1, source_target_pairs={{0,120},{8,0},{16,8},{24,16},{32,24},{40,32},{48,40},{56,48},{64,5... | collective-permute-start | bytes 614408 | tf_op jit(solution)/shard_map/ppermute | solution.py:254
  83.5 2.6 %shard_map.160 = (f32[128,768]{1,0:T(8,128)S(1)}, f32[2,768]{1,0:T(2,128)S(1)}) custom-call(bf16[128,768]{1,0:T(8,128)(2,1)S(1)} %shard_map.156.refs_0_, f32[1,768]{1,0:T(1,128)S(1)} %bitcast.27, bf16[2,400,128]{2,1,0:T(8,128)(2,1)S(1)} %collective-permute-done.9.refs_2_, ...), custom_call_target="tpu_custom_call", output_to_operand_aliasing={{0}: (4, {}), {1}: (5, {})} | custom-call | flops 314572800 | bytes 1408000 | tf_op jit(solution)/shard_map/pallas_call | solution.py:31
  86.0 1.2 collective-permute-done.11.refs_2_
  87.2 3.4 %collective-permute-start.16 = (bf16[2,400,128]{2,1,0:T(8,128)(2,1)S(1)}, bf16[2,400,128]{2,1,0:T(8,128)(2,1)S(1)}, u32[]{:S(2)}, u32[]{:S(2)}) collective-permute-start(bf16[2,400,128]{2,1,0:T(8,128)(2,1)S(1)} %collective-permute-done.14.refs_3_), channel_id=1, source_target_pairs={{0,120},{8,0},{16,8},{24,16},{32,24},{40,32},{48,40},{56,48},{64,5... | collective-permute-start | bytes 614408 | tf_op jit(solution)/shard_map/ppermute | solution.py:254
  90.6 2.6 %shard_map.161 = (f32[128,768]{1,0:T(8,128)S(1)}, f32[2,768]{1,0:T(2,128)S(1)}) custom-call(bf16[128,768]{1,0:T(8,128)(2,1)S(1)} %shard_map.156.refs_0_, f32[1,768]{1,0:T(1,128)S(1)} %bitcast.28, bf16[2,400,128]{2,1,0:T(8,128)(2,1)S(1)} %collective-permute-done.11.refs_2_, ...), custom_call_target="tpu_custom_call", output_to_operand_aliasing={{0}: (4, {}), {1}: (5, {})} | custom-call | flops 314572800 | bytes 1408000 | tf_op jit(solution)/shard_map/pallas_call | solution.py:31
  93.2 2.0 %collective-permute-done.13.refs_2_ = bf16[2,400,128]{2,1,0:T(8,128)(2,1)S(1)} collective-permute-done((bf16[2,400,128]{2,1,0:T(8,128)(2,1)S(1)}, bf16[2,400,128]{2,1,0:T(8,128)(2,1)S(1)}, u32[]{:S(2)}, u32[]{:S(2)}) %collective-permute-start.13) | collective-permute-done | bytes 204832 | tf_op jit(solution)/shard_map/ppermute | solution.py:254
  95.2 3.7 %collective-permute-start.18 = (bf16[2,400,128]{2,1,0:T(8,128)(2,1)S(1)}, bf16[2,400,128]{2,1,0:T(8,128)(2,1)S(1)}, u32[]{:S(2)}, u32[]{:S(2)}) collective-permute-start(bf16[2,400,128]{2,1,0:T(8,128)(2,1)S(1)} %collective-permute-done.16.refs_3_), channel_id=1, source_target_pairs={{0,120},{8,0},{16,8},{24,16},{32,24},{40,32},{48,40},{56,48},{64,5... | collective-permute-start | bytes 614408 | tf_op jit(solution)/shard_map/ppermute | solution.py:254
  98.9 2.6 %shard_map.162 = (f32[128,768]{1,0:T(8,128)S(1)}, f32[2,768]{1,0:T(2,128)S(1)}) custom-call(bf16[128,768]{1,0:T(8,128)(2,1)S(1)} %shard_map.156.refs_0_, f32[1,768]{1,0:T(1,128)S(1)} %bitcast.29, bf16[2,400,128]{2,1,0:T(8,128)(2,1)S(1)} %collective-permute-done.13.refs_2_, ...), custom_call_target="tpu_custom_call", output_to_operand_aliasing={{0}: (4, {}), {1}: (5, {})} | custom-call | flops 314572800 | bytes 1408000 | tf_op jit(solution)/shard_map/pallas_call | solution.py:31
  101.5 0.7 collective-permute-done.15.refs_2_
  102.2 0.9 collective-permute-done.18.refs_3_
  103.1 3.7 %collective-permute-start.20 = (bf16[2,400,128]{2,1,0:T(8,128)(2,1)S(1)}, bf16[2,400,128]{2,1,0:T(8,128)(2,1)S(1)}, u32[]{:S(2)}, u32[]{:S(2)}) collective-permute-start(bf16[2,400,128]{2,1,0:T(8,128)(2,1)S(1)} %collective-permute-done.18.refs_3_), channel_id=1, source_target_pairs={{0,120},{8,0},{16,8},{24,16},{32,24},{40,32},{48,40},{56,48},{64,5... | collective-permute-start | bytes 614408 | tf_op jit(solution)/shard_map/ppermute | solution.py:254
  106.8 2.6 %shard_map.163 = (f32[128,768]{1,0:T(8,128)S(1)}, f32[2,768]{1,0:T(2,128)S(1)}) custom-call(bf16[128,768]{1,0:T(8,128)(2,1)S(1)} %shard_map.156.refs_0_, f32[1,768]{1,0:T(1,128)S(1)} %bitcast.30, bf16[2,400,128]{2,1,0:T(8,128)(2,1)S(1)} %collective-permute-done.15.refs_2_, ...), custom_call_target="tpu_custom_call", output_to_operand_aliasing={{0}: (4, {}), {1}: (5, {})} | custom-call | flops 314572800 | bytes 1408000 | tf_op jit(solution)/shard_map/pallas_call | solution.py:31
  109.4 0.7 collective-permute-done.20.refs_3_
  110.1 3.8 %collective-permute-start.21 = (bf16[400,128]{1,0:T(8,128)(2,1)S(1)}, bf16[400,128]{1,0:T(8,128)(2,1)S(1)}, u32[]{:S(2)}, u32[]{:S(2)}) collective-permute-start(bf16[400,128]{1,0:T(8,128)(2,1)S(1)} %slice_bitcast_fusion), channel_id=1, source_target_pairs={{0,120},{8,0},{16,8},{24,16},{32,24},{40,32},{48,40},{56,48},{64,5... | collective-permute-start | bytes 307208 | tf_op jit(solution)/shard_map/ppermute | solution.py:254
  113.9 0.4 collective-permute-start.19
  114.3 2.6 %shard_map.164 = (f32[128,768]{1,0:T(8,128)S(1)}, f32[2,768]{1,0:T(2,128)S(1)}, bf16[1024,2048]{1,0:T(8,128)(2,1)S(1)}) custom-call(bf16[1024,2048]{1,0:T(8,128)(2,1)} %source.1, bf16[128,768]{1,0:T(8,128)(2,1)S(1)} %shard_map.156.refs_0_, f32[1,768]{1,0:T(1,128)S(1)} %bitcast.31, ...), custom_call_target="tpu_custom_call", output_to_operand_aliasing={{0}: (5, {}), {1}: (6, {})} | custom-call | flops 314572800 | bytes 9796608 | tf_op jit(solution)/shard_map/pallas_call | solution.py:31
  116.9 3.2 %collective-permute-done.19.refs_2_ = bf16[400,128]{1,0:T(8,128)(2,1)S(1)} collective-permute-done((bf16[400,128]{1,0:T(8,128)(2,1)S(1)}, bf16[400,128]{1,0:T(8,128)(2,1)S(1)}, u32[]{:S(2)}, u32[]{:S(2)}) %collective-permute-start.19) | collective-permute-done | bytes 102432 | tf_op jit(solution)/shard_map/ppermute | solution.py:254
  120.1 1.5 %shard_map.165 = (f32[128,768]{1,0:T(8,128)S(1)}, f32[2,768]{1,0:T(2,128)S(1)}) custom-call(bf16[128,768]{1,0:T(8,128)(2,1)S(1)} %shard_map.156.refs_0_, f32[1,768]{1,0:T(1,128)S(1)} %bitcast.32, bf16[400,128]{1,0:T(8,128)(2,1)S(1)} %collective-permute-done.19.refs_2_, ...), custom_call_target="tpu_custom_call", output_to_operand_aliasing={{0}: (4, {}), {1}: (5, {})} | custom-call | flops 157286400 | bytes 1203200 | tf_op jit(solution)/shard_map/pallas_call | solution.py:31
  121.9 2.0 %collective-permute-start.23 = (bf16[96,256]{1,0:T(8,128)(2,1)S(1)}, bf16[96,256]{1,0:T(8,128)(2,1)S(1)}, u32[]{:S(2)}, u32[]{:S(2)}) collective-permute-start(bf16[96,256]{1,0:T(8,128)(2,1)S(1)} %get-tuple-element.144), channel_id=1, source_target_pairs={{0,2},{2,4},{4,6},{6,0},{1,3},{3,5},{5,7},{7,1},{8,10},{10,12},{12... | collective-permute-start | bytes 147464 | tf_op jit(solution)/shard_map/ppermute | solution.py:254
  124.2 1.8 %collective-permute-done.22.a1 = bf16[96,256]{1,0:T(8,128)(2,1)S(1)} collective-permute-done((bf16[96,256]{1,0:T(8,128)(2,1)S(1)}, bf16[96,256]{1,0:T(8,128)(2,1)S(1)}, u32[]{:S(2)}, u32[]{:S(2)}) %collective-permute-start.22) | collective-permute-done | bytes 49184 | tf_op jit(solution)/shard_map/ppermute | solution.py:254
  126.0 1.3 %collective-permute-done.23.a2 = bf16[96,256]{1,0:T(8,128)(2,1)S(1)} collective-permute-done((bf16[96,256]{1,0:T(8,128)(2,1)S(1)}, bf16[96,256]{1,0:T(8,128)(2,1)S(1)}, u32[]{:S(2)}, u32[]{:S(2)}) %collective-permute-start.23) | collective-permute-done | bytes 49184 | tf_op jit(solution)/shard_map/ppermute | solution.py:254
  127.3 2.2 %collective-permute-done.24.a3 = bf16[96,256]{1,0:T(8,128)(2,1)S(1)} collective-permute-done((bf16[96,256]{1,0:T(8,128)(2,1)S(1)}, bf16[96,256]{1,0:T(8,128)(2,1)S(1)}, u32[]{:S(2)}, u32[]{:S(2)}) %collective-permute-start.24) | collective-permute-done | bytes 49184 | tf_op jit(solution)/shard_map/ppermute | solution.py:254
  129.5 2.2 %shard_map.167 = bf16[96,2048]{1,0:T(8,128)(2,1)} custom-call(s32[4]{0:T(128)S(1)} %add_add_fusion.1.order, bf16[96,256]{1,0:T(8,128)(2,1)S(1)} %get-tuple-element.142.a0, bf16[96,256]{1,0:T(8,128)(2,1)S(1)} %collective-permute-done.22.a1, bf16[96,256]{1,0:T(8,128)(2,1)S(1)} %collective-permute-done.23.a2, bf16[96,256]{1,0:T(8,128)(2,1)S(1)} %collective-permute-done.24.a3, ...), custom_call_target="tpu_custom_call" | custom-call | flops 402653184 | bytes 5189648 | tf_op jit(solution)/shard_map/pallas_call | solution.py:31
  (54 shorter events, 1.3 us)
Async XLA Ops:
  0.0 33.1 %copy-start.9 = (f32[2]{0:T(128)S(1)}, f32[2]{0:T(128)}, u32[]{:S(2)}) copy-start(f32[2]{0:T(128)} %param.29) | copy-start | bytes 28
  0.0 49.5 %collective-permute-start = (bf16[96,2048]{1,0:T(8,128)(2,1)}, bf16[96,2048]{1,0:T(8,128)(2,1)S(1)}, u32[]{:S(2)}, u32[]{:S(2)}) collective-permute-start(bf16[96,2048]{1,0:T(8,128)(2,1)} %bitcast.18), channel_id=1, source_target_pairs={{0,2},{2,4},{4,6},{6,0},{1,3},{3,5},{5,7},{7,1},{8,10},{10,12},{12... | collective-permute-start | bytes 1179656 | tf_op jit(solution)/shard_map/ppermute | solution.py:254
  1.6 48.3 %collective-permute-start.1 = (bf16[96,2048]{1,0:T(8,128)(2,1)}, bf16[96,2048]{1,0:T(8,128)(2,1)}, u32[]{:S(2)}, u32[]{:S(2)}) collective-permute-start(bf16[96,2048]{1,0:T(8,128)(2,1)} %bitcast.19), channel_id=1, source_target_pairs={{0,6},{2,0},{4,2},{6,4},{1,7},{3,1},{5,3},{7,5},{8,14},{10,8},{12,... | collective-permute-start | bytes 1179656 | tf_op jit(solution)/shard_map/ppermute | solution.py:254
  3.3 46.6 %collective-permute-start.2 = (bf16[96,2048]{1,0:T(8,128)(2,1)}, bf16[96,2048]{1,0:T(8,128)(2,1)}, u32[]{:S(2)}, u32[]{:S(2)}) collective-permute-start(bf16[96,2048]{1,0:T(8,128)(2,1)} %bitcast.20), channel_id=1, source_target_pairs={{0,4},{2,6},{4,0},{6,2},{1,5},{3,7},{5,1},{7,3},{8,12},{10,14},{12... | collective-permute-start | bytes 1179656 | tf_op jit(solution)/shard_map/ppermute | solution.py:254
  7.3 38.8 %all-to-all-start = ((f32[16,4,640]{2,1,0:T(4,128)}), f32[16,4,640]{2,1,0:T(4,128)S(1)}, u32[]{:S(2)}, u32[]{:S(2)}) async-start(f32[16,4,640]{2,1,0:T(4,128)} %modulation.1), calls=%async_computation | async-start | bytes 327680 | tf_op jit(solution)/shard_map/all_to_all | solution.py:301
  31.6 2.0 %copy-start.6 = (bf16[2048,128]{1,0:T(8,128)(2,1)S(1)}, bf16[2048,128]{1,0:T(8,128)(2,1)}, u32[]{:S(2)}) copy-start(bf16[2048,128]{1,0:T(8,128)(2,1)} %param.26) | copy-start | bytes 1572868
  31.6 2.0 %copy-start.7 = (bf16[2048,128]{1,0:T(8,128)(2,1)S(1)}, bf16[2048,128]{1,0:T(8,128)(2,1)}, u32[]{:S(2)}) copy-start(bf16[2048,128]{1,0:T(8,128)(2,1)} %param.25) | copy-start | bytes 1572868
  33.1 16.8 %copy-start.8 = (f32[1024]{0:T(1024)S(1)}, f32[1024]{0:T(1024)}, u32[]{:S(2)}) copy-start(f32[1024]{0:T(1024)} %param.30) | copy-start | bytes 12292
  33.1 21.6 %copy-start = (bf16[1,96,2048]{2,1,0:T(8,128)(2,1)S(1)}, bf16[1,96,2048]{2,1,0:T(8,128)(2,1)}, u32[]{:S(2)}) copy-start(bf16[1,96,2048]{2,1,0:T(8,128)(2,1)} %param.16) | copy-start | bytes 1179652
  33.1 21.6 %copy-start.2 = (bf16[1,16,2048]{2,1,0:T(8,128)(2,1)S(1)}, bf16[1,16,2048]{2,1,0:T(8,128)(2,1)}, u32[]{:S(2)}) copy-start(bf16[1,16,2048]{2,1,0:T(8,128)(2,1)} %param.18) | copy-start | bytes 196612
  33.1 21.6 %copy-start.3 = (f32[2048]{0:T(1024)S(1)}, f32[2048]{0:T(1024)}, u32[]{:S(2)}) copy-start(f32[2048]{0:T(1024)} %param.23) | copy-start | bytes 24580
  33.1 21.6 %copy-start.4 = (f32[128]{0:T(128)S(1)}, f32[128]{0:T(128)}, u32[]{:S(2)}) copy-start(f32[128]{0:T(128)} %param.28) | copy-start | bytes 1540
  33.7 26.6 %copy-start.1 = (bf16[2048,256]{1,0:T(8,128)(2,1)S(1)}, bf16[2048,256]{1,0:T(8,128)(2,1)}, u32[]{:S(2)}) copy-start(bf16[2048,256]{1,0:T(8,128)(2,1)} %wq.1) | copy-start | bytes 3145732
  33.8 26.6 %copy-start.5 = (f32[128]{0:T(128)S(1)}, f32[128]{0:T(128)}, u32[]{:S(2)}) copy-start(f32[128]{0:T(128)} %param.27) | copy-start | bytes 1540
  46.1 5.0 %collective-permute-start.3 = (f32[4,640]{1,0:T(4,128)S(1)}, f32[4,640]{1,0:T(4,128)S(1)}, u32[]{:S(2)}, u32[]{:S(2)}) collective-permute-start(f32[4,640]{1,0:T(4,128)S(1)} %shard_map.154.m0), channel_id=1, source_target_pairs={{0,2},{2,4},{4,6},{6,0},{1,3},{3,5},{5,7},{7,1},{8,10},{10,12},{12... | collective-permute-start | bytes 30728 | tf_op jit(solution)/shard_map/ppermute | solution.py:254
  47.0 4.2 %collective-permute-start.4 = (f32[4,640]{1,0:T(4,128)S(1)}, f32[4,640]{1,0:T(4,128)S(1)}, u32[]{:S(2)}, u32[]{:S(2)}) collective-permute-start(f32[4,640]{1,0:T(4,128)S(1)} %shard_map.154.m0), channel_id=1, source_target_pairs={{0,6},{2,0},{4,2},{6,4},{1,7},{3,1},{5,3},{7,5},{8,14},{10,8},{12,... | collective-permute-start | bytes 30728 | tf_op jit(solution)/shard_map/ppermute | solution.py:254
  49.5 5.2 %collective-permute-start.5 = (f32[4,640]{1,0:T(4,128)S(1)}, f32[4,640]{1,0:T(4,128)S(1)}, u32[]{:S(2)}, u32[]{:S(2)}) collective-permute-start(f32[4,640]{1,0:T(4,128)S(1)} %shard_map.154.m0), channel_id=1, source_target_pairs={{0,4},{2,6},{4,0},{6,2},{1,5},{3,7},{5,1},{7,3},{8,12},{10,14},{12... | collective-permute-start | bytes 30728 | tf_op jit(solution)/shard_map/ppermute | solution.py:254
  57.0 8.6 %collective-permute-start.6 = (bf16[2,400,128]{2,1,0:T(8,128)(2,1)S(1)}, bf16[2,400,128]{2,1,0:T(8,128)(2,1)S(1)}, u32[]{:S(2)}, u32[]{:S(2)}) collective-permute-start(bf16[2,400,128]{2,1,0:T(8,128)(2,1)S(1)} %get-tuple-element.81.refs_2_), channel_id=1, source_target_pairs={{0,8},{8,16},{16,24},{24,32},{32,40},{40,48},{48,56},{56,64},{64,7... | collective-permute-start | bytes 614408 | tf_op jit(solution)/shard_map/ppermute | solution.py:254
  58.5 7.1 %collective-permute-start.8 = (bf16[2,400,128]{2,1,0:T(8,128)(2,1)S(1)}, bf16[2,400,128]{2,1,0:T(8,128)(2,1)S(1)}, u32[]{:S(2)}, u32[]{:S(2)}) collective-permute-start(bf16[2,400,128]{2,1,0:T(8,128)(2,1)S(1)} %get-tuple-element.81.refs_2_), channel_id=1, source_target_pairs={{0,120},{8,0},{16,8},{24,16},{32,24},{40,32},{48,40},{56,48},{64,5... | collective-permute-start | bytes 614408 | tf_op jit(solution)/shard_map/ppermute | solution.py:254
  65.6 7.6 %collective-permute-start.7 = (bf16[2,400,128]{2,1,0:T(8,128)(2,1)S(1)}, bf16[2,400,128]{2,1,0:T(8,128)(2,1)S(1)}, u32[]{:S(2)}, u32[]{:S(2)}) collective-permute-start(bf16[2,400,128]{2,1,0:T(8,128)(2,1)S(1)} %collective-permute-done.6.refs_2_), channel_id=1, source_target_pairs={{0,8},{8,16},{16,24},{24,32},{32,40},{40,48},{48,56},{56,64},{64,7... | collective-permute-start | bytes 614408 | tf_op jit(solution)/shard_map/ppermute | solution.py:254
  65.6 7.6 %collective-permute-start.10 = (bf16[2,400,128]{2,1,0:T(8,128)(2,1)S(1)}, bf16[2,400,128]{2,1,0:T(8,128)(2,1)S(1)}, u32[]{:S(2)}, u32[]{:S(2)}) collective-permute-start(bf16[2,400,128]{2,1,0:T(8,128)(2,1)S(1)} %collective-permute-done.8.refs_3_), channel_id=1, source_target_pairs={{0,120},{8,0},{16,8},{24,16},{32,24},{40,32},{48,40},{56,48},{64,5... | collective-permute-start | bytes 614408 | tf_op jit(solution)/shard_map/ppermute | solution.py:254
  73.3 7.0 %collective-permute-start.9 = (bf16[2,400,128]{2,1,0:T(8,128)(2,1)S(1)}, bf16[2,400,128]{2,1,0:T(8,128)(2,1)S(1)}, u32[]{:S(2)}, u32[]{:S(2)}) collective-permute-start(bf16[2,400,128]{2,1,0:T(8,128)(2,1)S(1)} %collective-permute-done.7.refs_2_), channel_id=1, source_target_pairs={{0,8},{8,16},{16,24},{24,32},{32,40},{40,48},{48,56},{56,64},{64,7... | collective-permute-start | bytes 614408 | tf_op jit(solution)/shard_map/ppermute | solution.py:254
  73.3 7.0 %collective-permute-start.12 = (bf16[2,400,128]{2,1,0:T(8,128)(2,1)S(1)}, bf16[2,400,128]{2,1,0:T(8,128)(2,1)S(1)}, u32[]{:S(2)}, u32[]{:S(2)}) collective-permute-start(bf16[2,400,128]{2,1,0:T(8,128)(2,1)S(1)} %collective-permute-done.10.refs_3_), channel_id=1, source_target_pairs={{0,120},{8,0},{16,8},{24,16},{32,24},{40,32},{48,40},{56,48},{64,5... | collective-permute-start | bytes 614408 | tf_op jit(solution)/shard_map/ppermute | solution.py:254
  80.2 7.0 %collective-permute-start.11 = (bf16[2,400,128]{2,1,0:T(8,128)(2,1)S(1)}, bf16[2,400,128]{2,1,0:T(8,128)(2,1)S(1)}, u32[]{:S(2)}, u32[]{:S(2)}) collective-permute-start(bf16[2,400,128]{2,1,0:T(8,128)(2,1)S(1)} %collective-permute-done.9.refs_2_), channel_id=1, source_target_pairs={{0,8},{8,16},{16,24},{24,32},{32,40},{40,48},{48,56},{56,64},{64,7... | collective-permute-start | bytes 614408 | tf_op jit(solution)/shard_map/ppermute | solution.py:254
  80.2 7.0 %collective-permute-start.14 = (bf16[2,400,128]{2,1,0:T(8,128)(2,1)S(1)}, bf16[2,400,128]{2,1,0:T(8,128)(2,1)S(1)}, u32[]{:S(2)}, u32[]{:S(2)}) collective-permute-start(bf16[2,400,128]{2,1,0:T(8,128)(2,1)S(1)} %collective-permute-done.12.refs_3_), channel_id=1, source_target_pairs={{0,120},{8,0},{16,8},{24,16},{32,24},{40,32},{48,40},{56,48},{64,5... | collective-permute-start | bytes 614408 | tf_op jit(solution)/shard_map/ppermute | solution.py:254
  87.2 8.0 %collective-permute-start.13 = (bf16[2,400,128]{2,1,0:T(8,128)(2,1)S(1)}, bf16[2,400,128]{2,1,0:T(8,128)(2,1)S(1)}, u32[]{:S(2)}, u32[]{:S(2)}) collective-permute-start(bf16[2,400,128]{2,1,0:T(8,128)(2,1)S(1)} %collective-permute-done.11.refs_2_), channel_id=1, source_target_pairs={{0,8},{8,16},{16,24},{24,32},{32,40},{40,48},{48,56},{56,64},{64,7... | collective-permute-start | bytes 614408 | tf_op jit(solution)/shard_map/ppermute | solution.py:254
  87.2 8.0 %collective-permute-start.16 = (bf16[2,400,128]{2,1,0:T(8,128)(2,1)S(1)}, bf16[2,400,128]{2,1,0:T(8,128)(2,1)S(1)}, u32[]{:S(2)}, u32[]{:S(2)}) collective-permute-start(bf16[2,400,128]{2,1,0:T(8,128)(2,1)S(1)} %collective-permute-done.14.refs_3_), channel_id=1, source_target_pairs={{0,120},{8,0},{16,8},{24,16},{32,24},{40,32},{48,40},{56,48},{64,5... | collective-permute-start | bytes 614408 | tf_op jit(solution)/shard_map/ppermute | solution.py:254
  95.2 7.0 %collective-permute-start.15 = (bf16[2,400,128]{2,1,0:T(8,128)(2,1)S(1)}, bf16[2,400,128]{2,1,0:T(8,128)(2,1)S(1)}, u32[]{:S(2)}, u32[]{:S(2)}) collective-permute-start(bf16[2,400,128]{2,1,0:T(8,128)(2,1)S(1)} %collective-permute-done.13.refs_2_), channel_id=1, source_target_pairs={{0,8},{8,16},{16,24},{24,32},{32,40},{40,48},{48,56},{56,64},{64,7... | collective-permute-start | bytes 614408 | tf_op jit(solution)/shard_map/ppermute | solution.py:254
  95.2 7.9 %collective-permute-start.18 = (bf16[2,400,128]{2,1,0:T(8,128)(2,1)S(1)}, bf16[2,400,128]{2,1,0:T(8,128)(2,1)S(1)}, u32[]{:S(2)}, u32[]{:S(2)}) collective-permute-start(bf16[2,400,128]{2,1,0:T(8,128)(2,1)S(1)} %collective-permute-done.16.refs_3_), channel_id=1, source_target_pairs={{0,120},{8,0},{16,8},{24,16},{32,24},{40,32},{48,40},{56,48},{64,5... | collective-permute-start | bytes 614408 | tf_op jit(solution)/shard_map/ppermute | solution.py:254
  102.2 7.2 %collective-permute-start.17 = (bf16[2,400,128]{2,1,0:T(8,128)(2,1)S(1)}, bf16[2,400,128]{2,1,0:T(8,128)(2,1)S(1)}, u32[]{:S(2)}, u32[]{:S(2)}) collective-permute-start(bf16[2,400,128]{2,1,0:T(8,128)(2,1)S(1)} %collective-permute-done.15.refs_2_), channel_id=1, source_target_pairs={{0,8},{8,16},{16,24},{24,32},{32,40},{40,48},{48,56},{56,64},{64,7... | collective-permute-start | bytes 614408 | tf_op jit(solution)/shard_map/ppermute | solution.py:254
  103.1 7.0 %collective-permute-start.20 = (bf16[2,400,128]{2,1,0:T(8,128)(2,1)S(1)}, bf16[2,400,128]{2,1,0:T(8,128)(2,1)S(1)}, u32[]{:S(2)}, u32[]{:S(2)}) collective-permute-start(bf16[2,400,128]{2,1,0:T(8,128)(2,1)S(1)} %collective-permute-done.18.refs_3_), channel_id=1, source_target_pairs={{0,120},{8,0},{16,8},{24,16},{32,24},{40,32},{48,40},{56,48},{64,5... | collective-permute-start | bytes 614408 | tf_op jit(solution)/shard_map/ppermute | solution.py:254
  110.1 6.8 %collective-permute-start.21 = (bf16[400,128]{1,0:T(8,128)(2,1)S(1)}, bf16[400,128]{1,0:T(8,128)(2,1)S(1)}, u32[]{:S(2)}, u32[]{:S(2)}) collective-permute-start(bf16[400,128]{1,0:T(8,128)(2,1)S(1)} %slice_bitcast_fusion), channel_id=1, source_target_pairs={{0,120},{8,0},{16,8},{24,16},{32,24},{40,32},{48,40},{56,48},{64,5... | collective-permute-start | bytes 307208 | tf_op jit(solution)/shard_map/ppermute | solution.py:254
  113.9 6.2 %collective-permute-start.19 = (bf16[400,128]{1,0:T(8,128)(2,1)S(1)}, bf16[400,128]{1,0:T(8,128)(2,1)S(1)}, u32[]{:S(2)}, u32[]{:S(2)}) collective-permute-start(bf16[400,128]{1,0:T(8,128)(2,1)S(1)} %slice_bitcast_fusion.1), channel_id=1, source_target_pairs={{0,8},{8,16},{16,24},{24,32},{32,40},{40,48},{48,56},{56,64},{64,7... | collective-permute-start | bytes 307208 | tf_op jit(solution)/shard_map/ppermute | solution.py:254
  121.8 4.2 %collective-permute-start.22 = (bf16[96,256]{1,0:T(8,128)(2,1)S(1)}, bf16[96,256]{1,0:T(8,128)(2,1)S(1)}, u32[]{:S(2)}, u32[]{:S(2)}) collective-permute-start(bf16[96,256]{1,0:T(8,128)(2,1)S(1)} %get-tuple-element.143), channel_id=1, source_target_pairs={{0,6},{2,0},{4,2},{6,4},{1,7},{3,1},{5,3},{7,5},{8,14},{10,8},{12,... | collective-permute-start | bytes 147464 | tf_op jit(solution)/shard_map/ppermute | solution.py:254
  121.9 5.4 %collective-permute-start.23 = (bf16[96,256]{1,0:T(8,128)(2,1)S(1)}, bf16[96,256]{1,0:T(8,128)(2,1)S(1)}, u32[]{:S(2)}, u32[]{:S(2)}) collective-permute-start(bf16[96,256]{1,0:T(8,128)(2,1)S(1)} %get-tuple-element.144), channel_id=1, source_target_pairs={{0,2},{2,4},{4,6},{6,0},{1,3},{3,5},{5,7},{7,1},{8,10},{10,12},{12... | collective-permute-start | bytes 147464 | tf_op jit(solution)/shard_map/ppermute | solution.py:254
  123.9 5.6 %collective-permute-start.24 = (bf16[96,256]{1,0:T(8,128)(2,1)S(1)}, bf16[96,256]{1,0:T(8,128)(2,1)S(1)}, u32[]{:S(2)}, u32[]{:S(2)}) collective-permute-start(bf16[96,256]{1,0:T(8,128)(2,1)S(1)} %get-tuple-element.145), channel_id=1, source_target_pairs={{0,4},{2,6},{4,0},{6,2},{1,5},{3,7},{5,1},{7,3},{8,12},{10,14},{12... | collective-permute-start | bytes 147464 | tf_op jit(solution)/shard_map/ppermute | solution.py:254

commit v2 on v1

--- a/solution.py
+++ b/solution.py
@@ -152,20 +152,13 @@
         out_ref[:, h * rows : (h + 1) * rows] = one.T.astype(BF16)
 
 
-def attend_kernel(ctx_rows, first, pairs, *refs):
-    refs = list(refs)
-    qt, lift = refs[0], refs[1]
-    if pairs:
-        chunks = [(refs[2], refs[3])]
-        rest = refs[4:]
+def attend_kernel(ctx_rows, first, *refs):
+    qt, lift, *refs = refs
+    if first:
+        *refs, acc_out, stat_out = refs
     else:
-        count = len(refs) - 2 - (2 if first else 4)
-        chunks = [(r.at[0], r.at[1]) for r in refs[2 : 2 + count]]
-        rest = refs[2 + count :]
-    if first:
-        acc_out, stat_out = rest
-    else:
-        acc_in, stat_in, acc_out, stat_out = rest
+        *refs, acc_in, stat_in, acc_out, stat_out = refs
+    chunks = [(r.at[0], r.at[1]) for r in refs]
     total = qt.shape[1]
     width = 256
 
@@ -337,18 +330,17 @@
     lanes = group * rows
     state_shapes = (shape((HEAD_DIM, lanes), F32), shape((2, lanes), F32))
     state = local_call(
-        functools.partial(attend_kernel, ctx_rows, True, False),
+        functools.partial(attend_kernel, ctx_rows, True),
         state_shapes,
         flops=4 * length * lanes * HEAD_DIM,
     )(qt, lift, chunk)
 
-    def attend(state, *chunks, pairs=False):
-        count = 1 if pairs else len(chunks)
+    def attend(state, *chunks):
         given = (qt, lift, *chunks, *state)
         return local_call(
-            functools.partial(attend_kernel, ctx_rows, False, pairs),
+            functools.partial(attend_kernel, ctx_rows, False),
             state_shapes,
-            flops=4 * count * length * lanes * HEAD_DIM,
+            flops=4 * len(chunks) * length * lanes * HEAD_DIM,
             aliases={len(given) - 2: 0, len(given) - 1: 1},
         )(*given)
 
@@ -361,19 +353,16 @@
         here_right, right, state = hop(right, 1, state)
         here_left, left, state = hop(left, -1, state)
         state = attend(state, here_right, here_left)
-    right, state = lax.optimization_barrier((right, state))
-    last_k = shifted(right[0], "sp", 1)
-    left, state = lax.optimization_barrier((left, state))
-    last_v = shifted(left[1], "sp", -1)
+    right, last, state = hop(right, 1, state)
     *state, w_kept = local_call(
-        functools.partial(keeping, functools.partial(attend_kernel, ctx_rows, False, False)),
+        functools.partial(keeping, functools.partial(attend_kernel, ctx_rows, False)),
         (*state_shapes, pltpu.VMEM(w_out.shape, BF16)),
         flops=8 * length * lanes * HEAD_DIM,
         specs=[FAR] + [space] * 6,
         scratch=[pltpu.SemaphoreType.DMA],
         aliases={5: 0, 6: 1},
     )(far(w_out), qt, lift, right, left, *state)
-    state = attend(state, last_k, last_v, pairs=True)
+    state = attend(state, last)
 
     own, to_left, to_right, to_far = local_call(
         finish_kernel, [shape((own_rows, q_cols), BF16)] * n_tp, flops=10**6

time: 132 us -> 130 us (0.985)
  starting transfers between devices: 63.4 us -> 58.8 us
  waiting for transfers between devices: 36.8 us -> 39.7 us
    ppermute x25 -> x24, starting transfers between devices: 39.4 us -> 34.8 us  [shifted(): return lax.ppermute(x, axis, [(i, (i + by) % count) for i in range(count)])]
    ppermute x25 -> x24, waiting for transfers between devices: 24.5 us -> 27.3 us  [shifted(): return lax.ppermute(x, axis, [(i, (i + by) % count) for i in range(count)])]
  transfers between devices with their start and end apart: 26 -> 25, of which waited for: 15 -> 14; matrix products, arithmetic and copies ran while one was open for 2% -> 2% of each run, Pallas kernels for 17% -> 17%
where the time goes in v2:
time: 130 us
  starting transfers between devices  58.8 us (45%)
  waiting for transfers between devices  39.7 us (31%)
  Pallas kernels  28.7 us (22%)
  other arithmetic  2.19 us (2%)
    ppermute x24, starting transfers between devices, shifted(): return lax.ppermute(x, axis, [(i, (i + by) % count) for i in range(count)])  34.8 us
    ppermute x24, waiting for transfers between devices, shifted(): return lax.ppermute(x, axis, [(i, (i + by) % count) for i in range(count)])  27.3 us
    pallas_call x14, Pallas kernels, run(): pl.pallas_call(body, out_shape=outs if single else tuple(shapes), in_spec...  26.7 us
    all_to_all x1, starting transfers between devices, on_device(): parts = lax.all_to_all(parts, 'sp', 0, 0)  24 us
    all_to_all x1, waiting for transfers between devices, on_device(): parts = lax.all_to_all(parts, 'sp', 0, 0)  12.3 us
  transfers between devices with their start and end apart: 25, of which 14 were waited for; matrix products, arithmetic and copies ran while one was open for 2% of the time, Pallas kernels for 17%

profile of v2, /device:TPU:40, one launch (start us, length us, event | category | flops | bytes accessed | tf_op | source)
XLA Modules:
  0.0 129.9 jit_solution(7649167527675017464)
XLA Ops:
  0.0 1.6 %collective-permute-start = (bf16[96,2048]{1,0:T(8,128)(2,1)}, bf16[96,2048]{1,0:T(8,128)(2,1)S(1)}, u32[]{:S(2)}, u32[]{:S(2)}) collective-permute-start(bf16[96,2048]{1,0:T(8,128)(2,1)} %bitcast.14), channel_id=1, source_target_pairs={{0,2},{2,4},{4,6},{6,0},{1,3},{3,5},{5,7},{7,1},{8,10},{10,12},{12... | collective-permute-start | bytes 1179656 | tf_op jit(solution)/shard_map/ppermute | solution.py:247
  1.6 1.6 %collective-permute-start.1 = (bf16[96,2048]{1,0:T(8,128)(2,1)}, bf16[96,2048]{1,0:T(8,128)(2,1)}, u32[]{:S(2)}, u32[]{:S(2)}) collective-permute-start(bf16[96,2048]{1,0:T(8,128)(2,1)} %bitcast.15), channel_id=1, source_target_pairs={{0,6},{2,0},{4,2},{6,4},{1,7},{3,1},{5,3},{7,5},{8,14},{10,8},{12,... | collective-permute-start | bytes 1179656 | tf_op jit(solution)/shard_map/ppermute | solution.py:247
  3.3 2.0 %collective-permute-start.2 = (bf16[96,2048]{1,0:T(8,128)(2,1)}, bf16[96,2048]{1,0:T(8,128)(2,1)}, u32[]{:S(2)}, u32[]{:S(2)}) collective-permute-start(bf16[96,2048]{1,0:T(8,128)(2,1)} %bitcast.16), channel_id=1, source_target_pairs={{0,4},{2,6},{4,0},{6,2},{1,5},{3,7},{5,1},{7,3},{8,12},{10,14},{12... | collective-permute-start | bytes 1179656 | tf_op jit(solution)/shard_map/ppermute | solution.py:247
  5.3 1.9 %modulation.1 = f32[16,4,640]{2,1,0:T(4,128)} custom-call(bf16[1,2048]{1,0:T(2,128)(2,1)} %cond.1, bf16[2048]{0:T(1024)(128)(2,1)} %cond_ctx.1, bf16[128,512]{1,0:T(8,128)(2,1)} %wa.1, bf16[128,512]{1,0:T(8,128)(2,1)} %wb.1, bf16[128,512]{1,0:T(8,128)(2,1)} %wc.1), custom_call_target="tpu_custom_call" | custom-call | flops 1000000 | bytes 1048576 | tf_op jit(solution)/shard_map/modulation/pallas_call | solution.py:278
  7.3 24.0 %all-to-all-start = ((f32[16,4,640]{2,1,0:T(4,128)}), f32[16,4,640]{2,1,0:T(4,128)S(1)}, u32[]{:S(2)}, u32[]{:S(2)}) async-start(f32[16,4,640]{2,1,0:T(4,128)} %modulation.1), calls=%async_computation | async-start | bytes 327680 | tf_op jit(solution)/shard_map/all_to_all | solution.py:294
  31.6 1.4 %fusion = (f32[384,32]{1,0:T(8,128)S(1)}, f32[384,32]{1,0:T(8,128)S(1)}, f32[384,32]{1,0:T(8,128)S(1)}, f32[384,32]{1,0:T(8,128)S(1)}, f32[384,32]{1,0:T(8,128)S(1)}, /*index=5*/f32[384,32]{1,0:T(8,128)S(1)}) fusion(f32[32]{0:T(128)S(1)} %multiply_power_fusion, f32[384]{0:T(512)S(1)} %get-tuple-element.151, f32[384]{0:T(512)S(1)} %get-tuple-element.152), kind=kLoop, calls=%fused_computation.7 | loop fusion | flops 49152 | bytes 298112 | tf_op jit(solution)/shard_map/neg | solution.py:241
  33.2 0.4 pad_maximum_fusion.1
  33.8 12.3 %all-to-all-done.parts = f32[16,4,640]{2,1,0:T(4,128)S(1)} async-done(((f32[16,4,640]{2,1,0:T(4,128)}), f32[16,4,640]{2,1,0:T(4,128)S(1)}, u32[]{:S(2)}, u32[]{:S(2)}) %all-to-all-start) | async-done | bytes 163872 | tf_op jit(solution)/shard_map/all_to_all | solution.py:294
  46.1 0.8 collective-permute-start.3
  47.0 2.5 %collective-permute-start.4 = (f32[4,640]{1,0:T(4,128)S(1)}, f32[4,640]{1,0:T(4,128)S(1)}, u32[]{:S(2)}, u32[]{:S(2)}) collective-permute-start(f32[4,640]{1,0:T(4,128)S(1)} %shard_map.154.m0), channel_id=1, source_target_pairs={{0,6},{2,0},{4,2},{6,4},{1,7},{3,1},{5,3},{7,5},{8,14},{10,8},{12,... | collective-permute-start | bytes 30728 | tf_op jit(solution)/shard_map/ppermute | solution.py:247
  49.5 0.3 collective-permute-start.5
  49.9 1.2 collective-permute-done.3.m1
  51.1 3.5 %collective-permute-done.5.m3 = f32[4,640]{1,0:T(4,128)S(1)} collective-permute-done((f32[4,640]{1,0:T(4,128)S(1)}, f32[4,640]{1,0:T(4,128)S(1)}, u32[]{:S(2)}, u32[]{:S(2)}) %collective-permute-start.5) | collective-permute-done | bytes 10272 | tf_op jit(solution)/shard_map/ppermute | solution.py:247
  54.7 2.3 %shard_map.155 = (bf16[2,400,128]{2,1,0:T(8,128)(2,1)S(1)}, bf16[400,2048]{1,0:T(8,128)(2,1)S(1)}, f32[1,2048]{1,0:T(1,128)S(1)}) custom-call(s32[4]{0:T(128)S(1)} %get-tuple-element.144.owners, bf16[96,2048]{1,0:T(8,128)(2,1)S(1)} %bitcast.17, bf16[96,2048]{1,0:T(8,128)(2,1)S(1)} %collective-permute-done.x1, bf16[96,2048]{1,0:T(8,128)(2,1)} %collective-permute-done.1.x2, ...), custom_call_target="tpu_custom_call" | custom-call | flops 419430400 | bytes 4981264 | tf_op jit(solution)/shard_map/pallas_call | solution.py:31
  57.0 1.5 %collective-permute-start.6 = (bf16[2,400,128]{2,1,0:T(8,128)(2,1)S(1)}, bf16[2,400,128]{2,1,0:T(8,128)(2,1)S(1)}, u32[]{:S(2)}, u32[]{:S(2)}) collective-permute-start(bf16[2,400,128]{2,1,0:T(8,128)(2,1)S(1)} %get-tuple-element.78.refs_2_), channel_id=1, source_target_pairs={{0,8},{8,16},{16,24},{24,32},{32,40},{40,48},{48,56},{56,64},{64,7... | collective-permute-start | bytes 614408 | tf_op jit(solution)/shard_map/ppermute | solution.py:247
  58.5 1.9 %collective-permute-start.8 = (bf16[2,400,128]{2,1,0:T(8,128)(2,1)S(1)}, bf16[2,400,128]{2,1,0:T(8,128)(2,1)S(1)}, u32[]{:S(2)}, u32[]{:S(2)}) collective-permute-start(bf16[2,400,128]{2,1,0:T(8,128)(2,1)S(1)} %get-tuple-element.78.refs_2_), channel_id=1, source_target_pairs={{0,120},{8,0},{16,8},{24,16},{32,24},{40,32},{48,40},{56,48},{64,5... | collective-permute-start | bytes 614408 | tf_op jit(solution)/shard_map/ppermute | solution.py:247
  60.4 1.1 shard_map.156.refs_0_
  61.5 1.5 %shard_map.157 = (f32[128,768]{1,0:T(8,128)S(1)}, f32[2,768]{1,0:T(2,128)S(1)}) custom-call(bf16[128,768]{1,0:T(8,128)(2,1)S(1)} %shard_map.156.refs_0_, f32[1,768]{1,0:T(1,128)S(1)} %bitcast.20, bf16[2,400,128]{2,1,0:T(8,128)(2,1)S(1)} %get-tuple-element.78.refs_2_), custom_call_target="tpu_custom_call" | custom-call | flops 157286400 | bytes 803840 | tf_op jit(solution)/shard_map/pallas_call | solution.py:31
  63.0 2.6 %collective-permute-done.6.refs_2_ = bf16[2,400,128]{2,1,0:T(8,128)(2,1)S(1)} collective-permute-done((bf16[2,400,128]{2,1,0:T(8,128)(2,1)S(1)}, bf16[2,400,128]{2,1,0:T(8,128)(2,1)S(1)}, u32[]{:S(2)}, u32[]{:S(2)}) %collective-permute-start.6) | collective-permute-done | bytes 204832 | tf_op jit(solution)/shard_map/ppermute | solution.py:247
  65.6 3.2 %collective-permute-start.10 = (bf16[2,400,128]{2,1,0:T(8,128)(2,1)S(1)}, bf16[2,400,128]{2,1,0:T(8,128)(2,1)S(1)}, u32[]{:S(2)}, u32[]{:S(2)}) collective-permute-start(bf16[2,400,128]{2,1,0:T(8,128)(2,1)S(1)} %collective-permute-done.8.refs_3_), channel_id=1, source_target_pairs={{0,120},{8,0},{16,8},{24,16},{32,24},{40,32},{48,40},{56,48},{64,5... | collective-permute-start | bytes 614408 | tf_op jit(solution)/shard_map/ppermute | solution.py:247
  68.9 2.6 %shard_map.158 = (f32[128,768]{1,0:T(8,128)S(1)}, f32[2,768]{1,0:T(2,128)S(1)}) custom-call(bf16[128,768]{1,0:T(8,128)(2,1)S(1)} %shard_map.156.refs_0_, f32[1,768]{1,0:T(1,128)S(1)} %bitcast.21, bf16[2,400,128]{2,1,0:T(8,128)(2,1)S(1)} %collective-permute-done.6.refs_2_, ...), custom_call_target="tpu_custom_call", output_to_operand_aliasing={{0}: (4, {}), {1}: (5, {})} | custom-call | flops 314572800 | bytes 1408000 | tf_op jit(solution)/shard_map/pallas_call | solution.py:31
  71.4 1.8 %collective-permute-done.7.refs_2_ = bf16[2,400,128]{2,1,0:T(8,128)(2,1)S(1)} collective-permute-done((bf16[2,400,128]{2,1,0:T(8,128)(2,1)S(1)}, bf16[2,400,128]{2,1,0:T(8,128)(2,1)S(1)}, u32[]{:S(2)}, u32[]{:S(2)}) %collective-permute-start.7) | collective-permute-done | bytes 204832 | tf_op jit(solution)/shard_map/ppermute | solution.py:247
  73.3 3.2 %collective-permute-start.12 = (bf16[2,400,128]{2,1,0:T(8,128)(2,1)S(1)}, bf16[2,400,128]{2,1,0:T(8,128)(2,1)S(1)}, u32[]{:S(2)}, u32[]{:S(2)}) collective-permute-start(bf16[2,400,128]{2,1,0:T(8,128)(2,1)S(1)} %collective-permute-done.10.refs_3_), channel_id=1, source_target_pairs={{0,120},{8,0},{16,8},{24,16},{32,24},{40,32},{48,40},{56,48},{64,5... | collective-permute-start | bytes 614408 | tf_op jit(solution)/shard_map/ppermute | solution.py:247
  76.5 2.6 %shard_map.159 = (f32[128,768]{1,0:T(8,128)S(1)}, f32[2,768]{1,0:T(2,128)S(1)}) custom-call(bf16[128,768]{1,0:T(8,128)(2,1)S(1)} %shard_map.156.refs_0_, f32[1,768]{1,0:T(1,128)S(1)} %bitcast.22, bf16[2,400,128]{2,1,0:T(8,128)(2,1)S(1)} %collective-permute-done.7.refs_2_, ...), custom_call_target="tpu_custom_call", output_to_operand_aliasing={{0}: (4, {}), {1}: (5, {})} | custom-call | flops 314572800 | bytes 1408000 | tf_op jit(solution)/shard_map/pallas_call | solution.py:31
  79.1 1.2 collective-permute-done.9.refs_2_
  80.2 3.2 %collective-permute-start.14 = (bf16[2,400,128]{2,1,0:T(8,128)(2,1)S(1)}, bf16[2,400,128]{2,1,0:T(8,128)(2,1)S(1)}, u32[]{:S(2)}, u32[]{:S(2)}) collective-permute-start(bf16[2,400,128]{2,1,0:T(8,128)(2,1)S(1)} %collective-permute-done.12.refs_3_), channel_id=1, source_target_pairs={{0,120},{8,0},{16,8},{24,16},{32,24},{40,32},{48,40},{56,48},{64,5... | collective-permute-start | bytes 614408 | tf_op jit(solution)/shard_map/ppermute | solution.py:247
  83.5 2.6 %shard_map.160 = (f32[128,768]{1,0:T(8,128)S(1)}, f32[2,768]{1,0:T(2,128)S(1)}) custom-call(bf16[128,768]{1,0:T(8,128)(2,1)S(1)} %shard_map.156.refs_0_, f32[1,768]{1,0:T(1,128)S(1)} %bitcast.23, bf16[2,400,128]{2,1,0:T(8,128)(2,1)S(1)} %collective-permute-done.9.refs_2_, ...), custom_call_target="tpu_custom_call", output_to_operand_aliasing={{0}: (4, {}), {1}: (5, {})} | custom-call | flops 314572800 | bytes 1408000 | tf_op jit(solution)/shard_map/pallas_call | solution.py:31
  86.0 1.2 collective-permute-done.11.refs_2_
  87.2 3.4 %collective-permute-start.16 = (bf16[2,400,128]{2,1,0:T(8,128)(2,1)S(1)}, bf16[2,400,128]{2,1,0:T(8,128)(2,1)S(1)}, u32[]{:S(2)}, u32[]{:S(2)}) collective-permute-start(bf16[2,400,128]{2,1,0:T(8,128)(2,1)S(1)} %collective-permute-done.14.refs_3_), channel_id=1, source_target_pairs={{0,120},{8,0},{16,8},{24,16},{32,24},{40,32},{48,40},{56,48},{64,5... | collective-permute-start | bytes 614408 | tf_op jit(solution)/shard_map/ppermute | solution.py:247
  90.6 2.6 %shard_map.161 = (f32[128,768]{1,0:T(8,128)S(1)}, f32[2,768]{1,0:T(2,128)S(1)}) custom-call(bf16[128,768]{1,0:T(8,128)(2,1)S(1)} %shard_map.156.refs_0_, f32[1,768]{1,0:T(1,128)S(1)} %bitcast.24, bf16[2,400,128]{2,1,0:T(8,128)(2,1)S(1)} %collective-permute-done.11.refs_2_, ...), custom_call_target="tpu_custom_call", output_to_operand_aliasing={{0}: (4, {}), {1}: (5, {})} | custom-call | flops 314572800 | bytes 1408000 | tf_op jit(solution)/shard_map/pallas_call | solution.py:31
  93.2 2.0 %collective-permute-done.13.refs_2_ = bf16[2,400,128]{2,1,0:T(8,128)(2,1)S(1)} collective-permute-done((bf16[2,400,128]{2,1,0:T(8,128)(2,1)S(1)}, bf16[2,400,128]{2,1,0:T(8,128)(2,1)S(1)}, u32[]{:S(2)}, u32[]{:S(2)}) %collective-permute-start.13) | collective-permute-done | bytes 204832 | tf_op jit(solution)/shard_map/ppermute | solution.py:247
  95.2 3.7 %collective-permute-start.18 = (bf16[2,400,128]{2,1,0:T(8,128)(2,1)S(1)}, bf16[2,400,128]{2,1,0:T(8,128)(2,1)S(1)}, u32[]{:S(2)}, u32[]{:S(2)}) collective-permute-start(bf16[2,400,128]{2,1,0:T(8,128)(2,1)S(1)} %collective-permute-done.16.refs_3_), channel_id=1, source_target_pairs={{0,120},{8,0},{16,8},{24,16},{32,24},{40,32},{48,40},{56,48},{64,5... | collective-permute-start | bytes 614408 | tf_op jit(solution)/shard_map/ppermute | solution.py:247
  98.9 2.6 %shard_map.162 = (f32[128,768]{1,0:T(8,128)S(1)}, f32[2,768]{1,0:T(2,128)S(1)}) custom-call(bf16[128,768]{1,0:T(8,128)(2,1)S(1)} %shard_map.156.refs_0_, f32[1,768]{1,0:T(1,128)S(1)} %bitcast.25, bf16[2,400,128]{2,1,0:T(8,128)(2,1)S(1)} %collective-permute-done.13.refs_2_, ...), custom_call_target="tpu_custom_call", output_to_operand_aliasing={{0}: (4, {}), {1}: (5, {})} | custom-call | flops 314572800 | bytes 1408000 | tf_op jit(solution)/shard_map/pallas_call | solution.py:31
  101.5 2.9 %collective-permute-done.15.refs_2_ = bf16[2,400,128]{2,1,0:T(8,128)(2,1)S(1)} collective-permute-done((bf16[2,400,128]{2,1,0:T(8,128)(2,1)S(1)}, bf16[2,400,128]{2,1,0:T(8,128)(2,1)S(1)}, u32[]{:S(2)}, u32[]{:S(2)}) %collective-permute-start.15) | collective-permute-done | bytes 204832 | tf_op jit(solution)/shard_map/ppermute | solution.py:247
  104.4 3.2 %collective-permute-start.20 = (bf16[2,400,128]{2,1,0:T(8,128)(2,1)S(1)}, bf16[2,400,128]{2,1,0:T(8,128)(2,1)S(1)}, u32[]{:S(2)}, u32[]{:S(2)}) collective-permute-start(bf16[2,400,128]{2,1,0:T(8,128)(2,1)S(1)} %collective-permute-done.18.refs_3_), channel_id=1, source_target_pairs={{0,120},{8,0},{16,8},{24,16},{32,24},{40,32},{48,40},{56,48},{64,5... | collective-permute-start | bytes 614408 | tf_op jit(solution)/shard_map/ppermute | solution.py:247
  107.6 2.6 %shard_map.163 = (f32[128,768]{1,0:T(8,128)S(1)}, f32[2,768]{1,0:T(2,128)S(1)}) custom-call(bf16[128,768]{1,0:T(8,128)(2,1)S(1)} %shard_map.156.refs_0_, f32[1,768]{1,0:T(1,128)S(1)} %bitcast.26, bf16[2,400,128]{2,1,0:T(8,128)(2,1)S(1)} %collective-permute-done.15.refs_2_, ...), custom_call_target="tpu_custom_call", output_to_operand_aliasing={{0}: (4, {}), {1}: (5, {})} | custom-call | flops 314572800 | bytes 1408000 | tf_op jit(solution)/shard_map/pallas_call | solution.py:31
  110.2 1.2 collective-permute-done.17.refs_2_
  111.3 2.6 %shard_map.164 = (f32[128,768]{1,0:T(8,128)S(1)}, f32[2,768]{1,0:T(2,128)S(1)}, bf16[1024,2048]{1,0:T(8,128)(2,1)S(1)}) custom-call(bf16[1024,2048]{1,0:T(8,128)(2,1)} %source.1, bf16[128,768]{1,0:T(8,128)(2,1)S(1)} %shard_map.156.refs_0_, f32[1,768]{1,0:T(1,128)S(1)} %bitcast.27, ...), custom_call_target="tpu_custom_call", output_to_operand_aliasing={{0}: (5, {}), {1}: (6, {})} | custom-call | flops 314572800 | bytes 9796608 | tf_op jit(solution)/shard_map/pallas_call | solution.py:31
  113.9 4.4 %collective-permute-done.19.refs_2_ = bf16[2,400,128]{2,1,0:T(8,128)(2,1)S(1)} collective-permute-done((bf16[2,400,128]{2,1,0:T(8,128)(2,1)S(1)}, bf16[2,400,128]{2,1,0:T(8,128)(2,1)S(1)}, u32[]{:S(2)}, u32[]{:S(2)}) %collective-permute-start.19) | collective-permute-done | bytes 204832 | tf_op jit(solution)/shard_map/ppermute | solution.py:247
  118.3 1.5 %shard_map.165 = (f32[128,768]{1,0:T(8,128)S(1)}, f32[2,768]{1,0:T(2,128)S(1)}) custom-call(bf16[128,768]{1,0:T(8,128)(2,1)S(1)} %shard_map.156.refs_0_, f32[1,768]{1,0:T(1,128)S(1)} %bitcast.28, bf16[2,400,128]{2,1,0:T(8,128)(2,1)S(1)} %collective-permute-done.19.refs_2_, ...), custom_call_target="tpu_custom_call", output_to_operand_aliasing={{0}: (3, {}), {1}: (4, {})} | custom-call | flops 157286400 | bytes 1203200 | tf_op jit(solution)/shard_map/pallas_call | solution.py:31
  119.8 0.1 shard_map.166
  119.9 0.1 collective-permute-start.21
  120.1 2.0 %collective-permute-start.22 = (bf16[96,256]{1,0:T(8,128)(2,1)S(1)}, bf16[96,256]{1,0:T(8,128)(2,1)S(1)}, u32[]{:S(2)}, u32[]{:S(2)}) collective-permute-start(bf16[96,256]{1,0:T(8,128)(2,1)S(1)} %get-tuple-element.138), channel_id=1, source_target_pairs={{0,2},{2,4},{4,6},{6,0},{1,3},{3,5},{5,7},{7,1},{8,10},{10,12},{12... | collective-permute-start | bytes 147464 | tf_op jit(solution)/shard_map/ppermute | solution.py:247
  122.1 0.3 collective-permute-start.23
  122.4 1.8 %collective-permute-done.21.a1 = bf16[96,256]{1,0:T(8,128)(2,1)S(1)} collective-permute-done((bf16[96,256]{1,0:T(8,128)(2,1)S(1)}, bf16[96,256]{1,0:T(8,128)(2,1)S(1)}, u32[]{:S(2)}, u32[]{:S(2)}) %collective-permute-start.21) | collective-permute-done | bytes 49184 | tf_op jit(solution)/shard_map/ppermute | solution.py:247
  124.1 1.3 %collective-permute-done.22.a2 = bf16[96,256]{1,0:T(8,128)(2,1)S(1)} collective-permute-done((bf16[96,256]{1,0:T(8,128)(2,1)S(1)}, bf16[96,256]{1,0:T(8,128)(2,1)S(1)}, u32[]{:S(2)}, u32[]{:S(2)}) %collective-permute-start.22) | collective-permute-done | bytes 49184 | tf_op jit(solution)/shard_map/ppermute | solution.py:247
  125.5 2.2 %collective-permute-done.23.a3 = bf16[96,256]{1,0:T(8,128)(2,1)S(1)} collective-permute-done((bf16[96,256]{1,0:T(8,128)(2,1)S(1)}, bf16[96,256]{1,0:T(8,128)(2,1)S(1)}, u32[]{:S(2)}, u32[]{:S(2)}) %collective-permute-start.23) | collective-permute-done | bytes 49184 | tf_op jit(solution)/shard_map/ppermute | solution.py:247
  127.7 2.2 %shard_map.167 = bf16[96,2048]{1,0:T(8,128)(2,1)} custom-call(s32[4]{0:T(128)S(1)} %add_add_fusion.1.order, bf16[96,256]{1,0:T(8,128)(2,1)S(1)} %get-tuple-element.136.a0, bf16[96,256]{1,0:T(8,128)(2,1)S(1)} %collective-permute-done.21.a1, bf16[96,256]{1,0:T(8,128)(2,1)S(1)} %collective-permute-done.22.a2, bf16[96,256]{1,0:T(8,128)(2,1)S(1)} %collective-permute-done.23.a3, ...), custom_call_target="tpu_custom_call" | custom-call | flops 402653184 | bytes 5189648 | tf_op jit(solution)/shard_map/pallas_call | solution.py:31
  (50 shorter events, 0.7 us)
Async XLA Ops:
  0.0 33.1 %copy-start.9 = (f32[2]{0:T(128)S(1)}, f32[2]{0:T(128)}, u32[]{:S(2)}) copy-start(f32[2]{0:T(128)} %param.29) | copy-start | bytes 28
  0.0 49.5 %collective-permute-start = (bf16[96,2048]{1,0:T(8,128)(2,1)}, bf16[96,2048]{1,0:T(8,128)(2,1)S(1)}, u32[]{:S(2)}, u32[]{:S(2)}) collective-permute-start(bf16[96,2048]{1,0:T(8,128)(2,1)} %bitcast.14), channel_id=1, source_target_pairs={{0,2},{2,4},{4,6},{6,0},{1,3},{3,5},{5,7},{7,1},{8,10},{10,12},{12... | collective-permute-start | bytes 1179656 | tf_op jit(solution)/shard_map/ppermute | solution.py:247
  1.6 48.3 %collective-permute-start.1 = (bf16[96,2048]{1,0:T(8,128)(2,1)}, bf16[96,2048]{1,0:T(8,128)(2,1)}, u32[]{:S(2)}, u32[]{:S(2)}) collective-permute-start(bf16[96,2048]{1,0:T(8,128)(2,1)} %bitcast.15), channel_id=1, source_target_pairs={{0,6},{2,0},{4,2},{6,4},{1,7},{3,1},{5,3},{7,5},{8,14},{10,8},{12,... | collective-permute-start | bytes 1179656 | tf_op jit(solution)/shard_map/ppermute | solution.py:247
  3.3 46.6 %collective-permute-start.2 = (bf16[96,2048]{1,0:T(8,128)(2,1)}, bf16[96,2048]{1,0:T(8,128)(2,1)}, u32[]{:S(2)}, u32[]{:S(2)}) collective-permute-start(bf16[96,2048]{1,0:T(8,128)(2,1)} %bitcast.16), channel_id=1, source_target_pairs={{0,4},{2,6},{4,0},{6,2},{1,5},{3,7},{5,1},{7,3},{8,12},{10,14},{12... | collective-permute-start | bytes 1179656 | tf_op jit(solution)/shard_map/ppermute | solution.py:247
  7.3 38.8 %all-to-all-start = ((f32[16,4,640]{2,1,0:T(4,128)}), f32[16,4,640]{2,1,0:T(4,128)S(1)}, u32[]{:S(2)}, u32[]{:S(2)}) async-start(f32[16,4,640]{2,1,0:T(4,128)} %modulation.1), calls=%async_computation | async-start | bytes 327680 | tf_op jit(solution)/shard_map/all_to_all | solution.py:294
  31.6 2.0 %copy-start.6 = (bf16[2048,128]{1,0:T(8,128)(2,1)S(1)}, bf16[2048,128]{1,0:T(8,128)(2,1)}, u32[]{:S(2)}) copy-start(bf16[2048,128]{1,0:T(8,128)(2,1)} %param.26) | copy-start | bytes 1572868
  31.6 2.0 %copy-start.7 = (bf16[2048,128]{1,0:T(8,128)(2,1)S(1)}, bf16[2048,128]{1,0:T(8,128)(2,1)}, u32[]{:S(2)}) copy-start(bf16[2048,128]{1,0:T(8,128)(2,1)} %param.25) | copy-start | bytes 1572868
  33.1 16.8 %copy-start.8 = (f32[1024]{0:T(1024)S(1)}, f32[1024]{0:T(1024)}, u32[]{:S(2)}) copy-start(f32[1024]{0:T(1024)} %param.30) | copy-start | bytes 12292
  33.1 21.6 %copy-start = (bf16[1,96,2048]{2,1,0:T(8,128)(2,1)S(1)}, bf16[1,96,2048]{2,1,0:T(8,128)(2,1)}, u32[]{:S(2)}) copy-start(bf16[1,96,2048]{2,1,0:T(8,128)(2,1)} %param.16) | copy-start | bytes 1179652
  33.1 21.6 %copy-start.2 = (bf16[1,16,2048]{2,1,0:T(8,128)(2,1)S(1)}, bf16[1,16,2048]{2,1,0:T(8,128)(2,1)}, u32[]{:S(2)}) copy-start(bf16[1,16,2048]{2,1,0:T(8,128)(2,1)} %param.18) | copy-start | bytes 196612
  33.1 21.6 %copy-start.3 = (f32[2048]{0:T(1024)S(1)}, f32[2048]{0:T(1024)}, u32[]{:S(2)}) copy-start(f32[2048]{0:T(1024)} %param.23) | copy-start | bytes 24580
  33.1 21.6 %copy-start.4 = (f32[128]{0:T(128)S(1)}, f32[128]{0:T(128)}, u32[]{:S(2)}) copy-start(f32[128]{0:T(128)} %param.28) | copy-start | bytes 1540
  33.7 26.6 %copy-start.1 = (bf16[2048,256]{1,0:T(8,128)(2,1)S(1)}, bf16[2048,256]{1,0:T(8,128)(2,1)}, u32[]{:S(2)}) copy-start(bf16[2048,256]{1,0:T(8,128)(2,1)} %wq.1) | copy-start | bytes 3145732
  33.8 26.6 %copy-start.5 = (f32[128]{0:T(128)S(1)}, f32[128]{0:T(128)}, u32[]{:S(2)}) copy-start(f32[128]{0:T(128)} %param.27) | copy-start | bytes 1540
  46.1 5.0 %collective-permute-start.3 = (f32[4,640]{1,0:T(4,128)S(1)}, f32[4,640]{1,0:T(4,128)S(1)}, u32[]{:S(2)}, u32[]{:S(2)}) collective-permute-start(f32[4,640]{1,0:T(4,128)S(1)} %shard_map.154.m0), channel_id=1, source_target_pairs={{0,2},{2,4},{4,6},{6,0},{1,3},{3,5},{5,7},{7,1},{8,10},{10,12},{12... | collective-permute-start | bytes 30728 | tf_op jit(solution)/shard_map/ppermute | solution.py:247
  47.0 4.2 %collective-permute-start.4 = (f32[4,640]{1,0:T(4,128)S(1)}, f32[4,640]{1,0:T(4,128)S(1)}, u32[]{:S(2)}, u32[]{:S(2)}) collective-permute-start(f32[4,640]{1,0:T(4,128)S(1)} %shard_map.154.m0), channel_id=1, source_target_pairs={{0,6},{2,0},{4,2},{6,4},{1,7},{3,1},{5,3},{7,5},{8,14},{10,8},{12,... | collective-permute-start | bytes 30728 | tf_op jit(solution)/shard_map/ppermute | solution.py:247
  49.5 5.2 %collective-permute-start.5 = (f32[4,640]{1,0:T(4,128)S(1)}, f32[4,640]{1,0:T(4,128)S(1)}, u32[]{:S(2)}, u32[]{:S(2)}) collective-permute-start(f32[4,640]{1,0:T(4,128)S(1)} %shard_map.154.m0), channel_id=1, source_target_pairs={{0,4},{2,6},{4,0},{6,2},{1,5},{3,7},{5,1},{7,3},{8,12},{10,14},{12... | collective-permute-start | bytes 30728 | tf_op jit(solution)/shard_map/ppermute | solution.py:247
  57.0 8.6 %collective-permute-start.6 = (bf16[2,400,128]{2,1,0:T(8,128)(2,1)S(1)}, bf16[2,400,128]{2,1,0:T(8,128)(2,1)S(1)}, u32[]{:S(2)}, u32[]{:S(2)}) collective-permute-start(bf16[2,400,128]{2,1,0:T(8,128)(2,1)S(1)} %get-tuple-element.78.refs_2_), channel_id=1, source_target_pairs={{0,8},{8,16},{16,24},{24,32},{32,40},{40,48},{48,56},{56,64},{64,7... | collective-permute-start | bytes 614408 | tf_op jit(solution)/shard_map/ppermute | solution.py:247
  58.5 7.1 %collective-permute-start.8 = (bf16[2,400,128]{2,1,0:T(8,128)(2,1)S(1)}, bf16[2,400,128]{2,1,0:T(8,128)(2,1)S(1)}, u32[]{:S(2)}, u32[]{:S(2)}) collective-permute-start(bf16[2,400,128]{2,1,0:T(8,128)(2,1)S(1)} %get-tuple-element.78.refs_2_), channel_id=1, source_target_pairs={{0,120},{8,0},{16,8},{24,16},{32,24},{40,32},{48,40},{56,48},{64,5... | collective-permute-start | bytes 614408 | tf_op jit(solution)/shard_map/ppermute | solution.py:247
  65.6 7.6 %collective-permute-start.7 = (bf16[2,400,128]{2,1,0:T(8,128)(2,1)S(1)}, bf16[2,400,128]{2,1,0:T(8,128)(2,1)S(1)}, u32[]{:S(2)}, u32[]{:S(2)}) collective-permute-start(bf16[2,400,128]{2,1,0:T(8,128)(2,1)S(1)} %collective-permute-done.6.refs_2_), channel_id=1, source_target_pairs={{0,8},{8,16},{16,24},{24,32},{32,40},{40,48},{48,56},{56,64},{64,7... | collective-permute-start | bytes 614408 | tf_op jit(solution)/shard_map/ppermute | solution.py:247
  65.6 7.6 %collective-permute-start.10 = (bf16[2,400,128]{2,1,0:T(8,128)(2,1)S(1)}, bf16[2,400,128]{2,1,0:T(8,128)(2,1)S(1)}, u32[]{:S(2)}, u32[]{:S(2)}) collective-permute-start(bf16[2,400,128]{2,1,0:T(8,128)(2,1)S(1)} %collective-permute-done.8.refs_3_), channel_id=1, source_target_pairs={{0,120},{8,0},{16,8},{24,16},{32,24},{40,32},{48,40},{56,48},{64,5... | collective-permute-start | bytes 614408 | tf_op jit(solution)/shard_map/ppermute | solution.py:247
  73.3 7.0 %collective-permute-start.9 = (bf16[2,400,128]{2,1,0:T(8,128)(2,1)S(1)}, bf16[2,400,128]{2,1,0:T(8,128)(2,1)S(1)}, u32[]{:S(2)}, u32[]{:S(2)}) collective-permute-start(bf16[2,400,128]{2,1,0:T(8,128)(2,1)S(1)} %collective-permute-done.7.refs_2_), channel_id=1, source_target_pairs={{0,8},{8,16},{16,24},{24,32},{32,40},{40,48},{48,56},{56,64},{64,7... | collective-permute-start | bytes 614408 | tf_op jit(solution)/shard_map/ppermute | solution.py:247
  73.3 7.0 %collective-permute-start.12 = (bf16[2,400,128]{2,1,0:T(8,128)(2,1)S(1)}, bf16[2,400,128]{2,1,0:T(8,128)(2,1)S(1)}, u32[]{:S(2)}, u32[]{:S(2)}) collective-permute-start(bf16[2,400,128]{2,1,0:T(8,128)(2,1)S(1)} %collective-permute-done.10.refs_3_), channel_id=1, source_target_pairs={{0,120},{8,0},{16,8},{24,16},{32,24},{40,32},{48,40},{56,48},{64,5... | collective-permute-start | bytes 614408 | tf_op jit(solution)/shard_map/ppermute | solution.py:247
  80.2 7.0 %collective-permute-start.11 = (bf16[2,400,128]{2,1,0:T(8,128)(2,1)S(1)}, bf16[2,400,128]{2,1,0:T(8,128)(2,1)S(1)}, u32[]{:S(2)}, u32[]{:S(2)}) collective-permute-start(bf16[2,400,128]{2,1,0:T(8,128)(2,1)S(1)} %collective-permute-done.9.refs_2_), channel_id=1, source_target_pairs={{0,8},{8,16},{16,24},{24,32},{32,40},{40,48},{48,56},{56,64},{64,7... | collective-permute-start | bytes 614408 | tf_op jit(solution)/shard_map/ppermute | solution.py:247
  80.2 7.0 %collective-permute-start.14 = (bf16[2,400,128]{2,1,0:T(8,128)(2,1)S(1)}, bf16[2,400,128]{2,1,0:T(8,128)(2,1)S(1)}, u32[]{:S(2)}, u32[]{:S(2)}) collective-permute-start(bf16[2,400,128]{2,1,0:T(8,128)(2,1)S(1)} %collective-permute-done.12.refs_3_), channel_id=1, source_target_pairs={{0,120},{8,0},{16,8},{24,16},{32,24},{40,32},{48,40},{56,48},{64,5... | collective-permute-start | bytes 614408 | tf_op jit(solution)/shard_map/ppermute | solution.py:247
  87.2 8.0 %collective-permute-start.13 = (bf16[2,400,128]{2,1,0:T(8,128)(2,1)S(1)}, bf16[2,400,128]{2,1,0:T(8,128)(2,1)S(1)}, u32[]{:S(2)}, u32[]{:S(2)}) collective-permute-start(bf16[2,400,128]{2,1,0:T(8,128)(2,1)S(1)} %collective-permute-done.11.refs_2_), channel_id=1, source_target_pairs={{0,8},{8,16},{16,24},{24,32},{32,40},{40,48},{48,56},{56,64},{64,7... | collective-permute-start | bytes 614408 | tf_op jit(solution)/shard_map/ppermute | solution.py:247
  87.2 8.0 %collective-permute-start.16 = (bf16[2,400,128]{2,1,0:T(8,128)(2,1)S(1)}, bf16[2,400,128]{2,1,0:T(8,128)(2,1)S(1)}, u32[]{:S(2)}, u32[]{:S(2)}) collective-permute-start(bf16[2,400,128]{2,1,0:T(8,128)(2,1)S(1)} %collective-permute-done.14.refs_3_), channel_id=1, source_target_pairs={{0,120},{8,0},{16,8},{24,16},{32,24},{40,32},{48,40},{56,48},{64,5... | collective-permute-start | bytes 614408 | tf_op jit(solution)/shard_map/ppermute | solution.py:247
  95.2 9.2 %collective-permute-start.15 = (bf16[2,400,128]{2,1,0:T(8,128)(2,1)S(1)}, bf16[2,400,128]{2,1,0:T(8,128)(2,1)S(1)}, u32[]{:S(2)}, u32[]{:S(2)}) collective-permute-start(bf16[2,400,128]{2,1,0:T(8,128)(2,1)S(1)} %collective-permute-done.13.refs_2_), channel_id=1, source_target_pairs={{0,8},{8,16},{16,24},{24,32},{32,40},{40,48},{48,56},{56,64},{64,7... | collective-permute-start | bytes 614408 | tf_op jit(solution)/shard_map/ppermute | solution.py:247
  95.2 9.2 %collective-permute-start.18 = (bf16[2,400,128]{2,1,0:T(8,128)(2,1)S(1)}, bf16[2,400,128]{2,1,0:T(8,128)(2,1)S(1)}, u32[]{:S(2)}, u32[]{:S(2)}) collective-permute-start(bf16[2,400,128]{2,1,0:T(8,128)(2,1)S(1)} %collective-permute-done.16.refs_3_), channel_id=1, source_target_pairs={{0,120},{8,0},{16,8},{24,16},{32,24},{40,32},{48,40},{56,48},{64,5... | collective-permute-start | bytes 614408 | tf_op jit(solution)/shard_map/ppermute | solution.py:247
  104.4 7.0 %collective-permute-start.17 = (bf16[2,400,128]{2,1,0:T(8,128)(2,1)S(1)}, bf16[2,400,128]{2,1,0:T(8,128)(2,1)S(1)}, u32[]{:S(2)}, u32[]{:S(2)}) collective-permute-start(bf16[2,400,128]{2,1,0:T(8,128)(2,1)S(1)} %collective-permute-done.15.refs_2_), channel_id=1, source_target_pairs={{0,8},{8,16},{16,24},{24,32},{32,40},{40,48},{48,56},{56,64},{64,7... | collective-permute-start | bytes 614408 | tf_op jit(solution)/shard_map/ppermute | solution.py:247
  104.4 7.0 %collective-permute-start.20 = (bf16[2,400,128]{2,1,0:T(8,128)(2,1)S(1)}, bf16[2,400,128]{2,1,0:T(8,128)(2,1)S(1)}, u32[]{:S(2)}, u32[]{:S(2)}) collective-permute-start(bf16[2,400,128]{2,1,0:T(8,128)(2,1)S(1)} %collective-permute-done.18.refs_3_), channel_id=1, source_target_pairs={{0,120},{8,0},{16,8},{24,16},{32,24},{40,32},{48,40},{56,48},{64,5... | collective-permute-start | bytes 614408 | tf_op jit(solution)/shard_map/ppermute | solution.py:247
  111.3 7.0 %collective-permute-start.19 = (bf16[2,400,128]{2,1,0:T(8,128)(2,1)S(1)}, bf16[2,400,128]{2,1,0:T(8,128)(2,1)S(1)}, u32[]{:S(2)}, u32[]{:S(2)}) collective-permute-start(bf16[2,400,128]{2,1,0:T(8,128)(2,1)S(1)} %collective-permute-done.17.refs_2_), channel_id=1, source_target_pairs={{0,8},{8,16},{16,24},{24,32},{32,40},{40,48},{48,56},{56,64},{64,7... | collective-permute-start | bytes 614408 | tf_op jit(solution)/shard_map/ppermute | solution.py:247
  119.9 4.2 %collective-permute-start.21 = (bf16[96,256]{1,0:T(8,128)(2,1)S(1)}, bf16[96,256]{1,0:T(8,128)(2,1)S(1)}, u32[]{:S(2)}, u32[]{:S(2)}) collective-permute-start(bf16[96,256]{1,0:T(8,128)(2,1)S(1)} %get-tuple-element.137), channel_id=1, source_target_pairs={{0,6},{2,0},{4,2},{6,4},{1,7},{3,1},{5,3},{7,5},{8,14},{10,8},{12,... | collective-permute-start | bytes 147464 | tf_op jit(solution)/shard_map/ppermute | solution.py:247
  120.1 5.4 %collective-permute-start.22 = (bf16[96,256]{1,0:T(8,128)(2,1)S(1)}, bf16[96,256]{1,0:T(8,128)(2,1)S(1)}, u32[]{:S(2)}, u32[]{:S(2)}) collective-permute-start(bf16[96,256]{1,0:T(8,128)(2,1)S(1)} %get-tuple-element.138), channel_id=1, source_target_pairs={{0,2},{2,4},{4,6},{6,0},{1,3},{3,5},{5,7},{7,1},{8,10},{10,12},{12... | collective-permute-start | bytes 147464 | tf_op jit(solution)/shard_map/ppermute | solution.py:247
  122.1 5.6 %collective-permute-start.23 = (bf16[96,256]{1,0:T(8,128)(2,1)S(1)}, bf16[96,256]{1,0:T(8,128)(2,1)S(1)}, u32[]{:S(2)}, u32[]{:S(2)}) collective-permute-start(bf16[96,256]{1,0:T(8,128)(2,1)S(1)} %get-tuple-element.139), channel_id=1, source_target_pairs={{0,4},{2,6},{4,0},{6,2},{1,5},{3,7},{5,1},{7,3},{8,12},{10,14},{12... | collective-permute-start | bytes 147464 | tf_op jit(solution)/shard_map/ppermute | solution.py:247
